TPU v7x, 512 devices: a 4x2x32 block of a 4x8x32 slice. The times are simulated.
512 devices in a mesh: grp: 2 (over y), kv: 32 (over z), tp: 8 (over x, core).
Axes of the slice: x: 4, y: 2, z: 32, core: 2. Of those that a mesh axis runs over, the one named last changes fastest.
The devices are a block of a 4x8x32 slice.
Arguments:
- tokens: bfloat16 [256, 4096], P('grp', 'kv'), parts along dimension 0, may hold values from -40 to 40
- lengths: int32 [256], P(('grp', 'kv')), parts along dimension 0, may hold values from 1 to 6, 320 in all
- conv_state_x: bfloat16 [256, 3, 4096], P(('grp', 'kv'), None, 'tp'), parts along dimension 0, may hold values from -6 to 6
- conv_state_bc: bfloat16 [256, 3, 2, 1024], P(('grp', 'kv'), None, None, 'tp'), parts along dimension 0, may hold values from -6 to 6
- ssm_state: float32 [256, 64, 64, 128], P(('grp', 'kv'), 'tp'), parts along dimension 0, may hold values from -0.6 to 0.6
- norm_gain: bfloat16 [4096], P('kv'), may hold values from 0.099609375 to 1.8984375
- w_gate: bfloat16 [4096, 4096], P('kv', 'tp'), may hold values from -0.09375 to 0.09375
- w_value: bfloat16 [4096, 4096], P('kv', 'tp'), may hold values from -0.09375 to 0.09375
- w_key: bfloat16 [4096, 1024], P('kv', 'tp'), may hold values from -0.09375 to 0.09375
- w_query: bfloat16 [4096, 1024], P('kv', 'tp'), may hold values from -0.09375 to 0.09375
- w_step: bfloat16 [4096, 64], P('kv', 'tp'), may hold values from -0.09375 to 0.09375
- step_bias: float32 [64], P('tp'), may hold values from -2 to 0
- decay_log: float32 [64], P('tp'), may hold values from -2 to 1
- conv_x: bfloat16 [4, 4096], P(None, 'tp'), may hold values from -3 to 3
- conv_bc: bfloat16 [4, 2, 1024], P(None, None, 'tp'), may hold values from -3 to 3
- inner_gain: bfloat16 [4096], P('tp'), may hold values from 0.099609375 to 1.8984375
- w_out: bfloat16 [4096, 4096], P('tp', 'kv'), may hold values from -0.09375 to 0.09375
- mlp_gain: bfloat16 [4096], P('kv'), may hold values from 0.099609375 to 1.8984375
- w_up: bfloat16 [4096, 16384], P('kv', 'tp'), may hold values from -0.09375 to 0.09375
- w_down: bfloat16 [16384, 4096], P('tp', 'kv'), may hold values from -0.046875 to 0.046875
Outputs:
- layer_out: bfloat16 [256, 4096], P('grp', 'kv'), parts along dimension 0
- next_state: float32 [256, 64, 64, 128], P(('grp', 'kv'), 'tp'), parts along dimension 0
There are 2 independent parts, one for each index of `grp`. A program takes and returns all parts, laid end to end along the dimension named above; an argument that names none is the same for every part. Nothing has to cross between parts.
All inputs are finite; a program needn't handle non-finite values. No bound on the sum of `lengths` on one device may be relied on, other than what follows from the above.
Results may differ from a plain program's by a relative error of at most 0.008.
Values may be sent and summed in bfloat16 or wider, within the bound.
No kernel may reach another device: no remote copies, remote signals or barrier semaphores. Data moves between devices by JAX's collectives and lax.ppermute only.
A program may use at most 64 MiB of HBM per device.

v0:
```python
import jax
import jax.numpy as jnp
from jax import lax
from jax.sharding import PartitionSpec as P

D = 4096
HEAD_DIM = 64
STATE = 128
CONV_WIDTH = 4
INNER = 4096


epsilon = 1e-06


def in_blocks(shard, dim, size):
    before, after = (shard.shape[:dim], shard.shape[dim + 1 :])
    return jnp.moveaxis(shard.reshape(*before, size, -1, *after), dim, 0)


def summed_on_arrival(shard, axis, dim):
    parts = in_blocks(shard, dim, lax.axis_size(axis))
    arrived = lax.all_to_all(parts, axis, split_axis=0, concat_axis=0, tiled=True)
    return arrived.sum(axis=0)


def in_one_piece(arrays, axis, dim, along):
    columns = [a.reshape(*a.shape[:along], -1) for a in arrays]
    both = jnp.concatenate(columns, axis=along)
    filled, at, finished = (summed_on_arrival(both, axis, dim), 0, [])
    for a, column in zip(arrays, columns):
        slab = filled[..., at : at + column.shape[along]]
        finished.append(slab.reshape(*slab.shape[:along], *a.shape[along:]))
        at += column.shape[along]
    return tuple(finished)


def from_everyone(shard, axis):
    copies = jnp.broadcast_to(shard, (lax.axis_size(axis), *shard.shape))
    return lax.all_to_all(copies, axis, split_axis=0, concat_axis=0, tiled=True)


def over_copies(shard, axis):
    return from_everyone(shard, axis).sum(axis=0)


def laid_out(parts, dim):
    shape = list(parts.shape[1:])
    shape[dim] *= parts.shape[0]
    return jnp.moveaxis(parts, 0, dim).reshape(shape)


def gathered_copies(shard, axis, dim):
    parts = from_everyone(shard, axis)
    return laid_out(parts, dim)


def causal_conv(state_rows, newest, conv_weights):
    extended = jnp.concatenate([state_rows, newest[:, None]], axis=1)
    conv_sum = extended[:, 0] * conv_weights[0].astype(jnp.float32)
    for offset in range(1, conv_weights.shape[0]):
        conv_sum = conv_sum + extended[:, offset] * conv_weights[offset].astype(jnp.float32)
    return jax.nn.silu(conv_sum)


def product(left, right):
    return jnp.dot(left, right, preferred_element_type=jnp.float32)


def per_device(
    tokens,
    lengths,
    conv_state_x,
    conv_state_bc,
    ssm_state,
    norm_gain,
    w_gate,
    w_value,
    w_key,
    w_query,
    w_step,
    step_bias,
    decay_log,
    conv_x,
    conv_bc,
    inner_gain,
    w_out,
    mlp_gain,
    w_up,
    w_down,
):
    head_count = w_step.shape[1]
    group_count = w_key.shape[1] // STATE
    per_group = head_count // group_count
    widened = tokens.astype(jnp.float32)
    scaled = (widened * norm_gain.astype(jnp.float32)).astype(jnp.bfloat16)
    gate_raw, value_raw, key_raw, query_raw, step_raw, squares = in_one_piece(
        (
            product(scaled, w_gate),
            product(scaled, w_value),
            product(scaled, w_key),
            product(scaled, w_query),
            product(scaled, w_step),
            jnp.sum(widened * widened, axis=1),
        ),
        "kv",
        0,
        1,
    )
    seq_count = gate_raw.shape[0]
    inverse = lax.rsqrt(squares / D + epsilon)[:, None]
    row_live = (
        jnp.arange(CONV_WIDTH - 1, dtype=jnp.int32)[None, :] >= CONV_WIDTH - 1 - lengths[:, None]
    ).astype(jnp.float32)
    live_x = conv_state_x.astype(jnp.float32) * row_live[:, :, None]
    live_bc = conv_state_bc.astype(jnp.float32) * row_live[:, :, None, None]
    mixed_values = causal_conv(live_x, value_raw * inverse, conv_x).reshape(
        seq_count, head_count, HEAD_DIM
    )
    key_query = causal_conv(
        live_bc, jnp.stack([key_raw * inverse, query_raw * inverse], axis=1), conv_bc
    )
    key_heads = jnp.repeat(
        key_query[:, 0].reshape(seq_count, group_count, STATE), per_group, axis=1
    )
    query_heads = jnp.repeat(
        key_query[:, 1].reshape(seq_count, group_count, STATE), per_group, axis=1
    )
    step_size = jax.nn.softplus(step_raw * inverse + step_bias)
    rate_now = -jnp.exp(decay_log) * step_size
    next_state = (
        ssm_state * jnp.exp(rate_now)[:, :, None, None]
        + (step_size[:, :, None] * mixed_values)[:, :, :, None] * key_heads[:, :, None, :]
    )
    mixer_y = jnp.einsum(
        "bhpn,bhn->bhp", next_state, query_heads, precision=lax.Precision.HIGHEST
    ).reshape(seq_count, head_count * HEAD_DIM)
    gated_rows = mixer_y * jax.nn.silu(gate_raw * inverse)
    gated_low = (gated_rows * inner_gain.astype(jnp.float32)).astype(jnp.bfloat16)
    all_low, all_squares = (
        lax.all_gather(gated_low, "kv", axis=0, tiled=True),
        lax.all_gather(
            jnp.sum(gated_rows * gated_rows, axis=1).astype(jnp.bfloat16), "kv", axis=0, tiled=True
        ).astype(jnp.float32),
    )
    out_sum, gated_total = (
        over_copies(product(all_low, w_out), "tp"),
        over_copies(all_squares, "tp"),
    )
    residual = (widened + out_sum * lax.rsqrt(gated_total / INNER + epsilon)[:, None]).astype(
        jnp.bfloat16
    )
    residual_wide = residual.astype(jnp.float32)
    hidden_low = (residual_wide * mlp_gain.astype(jnp.float32)).astype(jnp.bfloat16)
    row_squares = jnp.sum(residual_wide * residual_wide, axis=1)
    up_share, square_share = in_one_piece((product(hidden_low, w_up), row_squares), "kv", 0, 1)
    share_active = jnp.square(
        jax.nn.relu(up_share * lax.rsqrt(square_share / D + epsilon)[:, None])
    ).astype(jnp.bfloat16)
    activation = gathered_copies(share_active, "kv", 0)
    down_sum = over_copies(product(activation, w_down), "tp")
    layer_out = (residual_wide + down_sum).astype(jnp.bfloat16)
    return (layer_out, next_state)


def solution(mesh):
    return jax.shard_map(
        per_device,
        mesh=mesh,
        in_specs=(
            P("grp", "kv"),
            P(("grp", "kv")),
            P(("grp", "kv"), None, "tp"),
            P(("grp", "kv"), None, None, "tp"),
            P(("grp", "kv"), "tp", None, None),
            P("kv"),
            P("kv", "tp"),
            P("kv", "tp"),
            P("kv", "tp"),
            P("kv", "tp"),
            P("kv", "tp"),
            P("tp"),
            P("tp"),
            P(None, "tp"),
            P(None, None, "tp"),
            P("tp"),
            P("tp", "kv"),
            P("kv"),
            P("kv", "tp"),
            P("tp", "kv"),
        ),
        out_specs=(P("grp", "kv"), P(("grp", "kv"), "tp", None, None)),
        check_vma=False,
    )
```

profile of v0, /device:TPU:33, one launch (start us, length us, event | category | flops | bytes accessed | tf_op | source)
XLA Modules:
  0.0 471.4 jit_solution(15149226765499633924)
XLA Ops:
  0.7 0.7 convert_element_type.73
  1.4 0.9 fusion.1
  2.5 0.9 fusion.16
  3.4 0.9 fusion.14
  4.3 0.9 fusion.12
  5.2 1.1 fusion.18
  6.8 1.2 concatenate.30
  8.0 46.4 %all-to-all-start = ((f32[32,4,1289]{2,1,0:T(4,128)}), f32[32,4,1289]{2,1,0:T(4,128)S(1)}, u32[]{:S(2)}, u32[]{:S(2)}) async-start(f32[32,4,1289]{2,1,0:T(4,128)} %concatenate.30), calls=%async_computation | async-start | bytes 1441792 | tf_op jit(solution)/shard_map/all_to_all | solution.py:23
  54.4 1.3 dynamic-slice
  56.6 79.0 %all-to-all-done = f32[32,4,1289]{2,1,0:T(4,128)S(1)} async-done(((f32[32,4,1289]{2,1,0:T(4,128)}), f32[32,4,1289]{2,1,0:T(4,128)S(1)}, u32[]{:S(2)}, u32[]{:S(2)}) %all-to-all-start) | async-done | bytes 660000 | tf_op jit(solution)/shard_map/all_to_all | solution.py:23
  136.3 0.4 multiply_add_fusion
  136.8 1.7 fusion.49
  139.1 39.4 %all-reduce = bf16[128]{0:T(256)(128)(2,1)S(1)} all-reduce(bf16[128]{0:T(256)(128)(2,1)S(1)} %dynamic-update-slice), channel_id=1, replica_groups=mesh['grp'=2,'kv'=32,'tp'=8] {'kv'}, use_global_device_ids=true, to_apply=%add | all-reduce | flops 128 | bytes 512
  178.5 0.6 broadcast_in_dim.9
  179.1 18.6 %all-to-all-start.2 = ((f32[8,1,128]{2,1,0:T(1,128)}), f32[8,1,128]{2,1,0:T(1,128)S(1)}, u32[]{:S(2)}, u32[]{:S(2)}) async-start(f32[8,1,128]{2,1,0:T(1,128)} %broadcast_in_dim.9), calls=%async_computation.2 | async-start | bytes 8192 | tf_op jit(solution)/shard_map/all_to_all | solution.py:40
  197.7 40.2 %all-gather = bf16[32,4,512]{2,1,0:T(4,128)(2,1)S(1)} all-gather(bf16[1,4,512]{2,1,0:T(4,128)(2,1)S(1)} %fusion.30), channel_id=1, replica_groups=mesh['grp'=2,'kv'=32,'tp'=8] {'kv'}, dimensions={0}, use_global_device_ids=true | all-gather | bytes 135168 | tf_op jit(solution)/shard_map/all_gather | solution.py:141
  238.2 0.8 broadcast_in_dim.8
  239.0 18.5 %all-to-all-start.1 = ((f32[8,128,128]{2,1,0:T(8,128)}), f32[8,128,128]{2,1,0:T(8,128)S(1)}, u32[]{:S(2)}, u32[]{:S(2)}) async-start(f32[8,128,128]{2,1,0:T(8,128)} %broadcast_in_dim.8), calls=%async_computation.1 | async-start | bytes 1048576 | tf_op jit(solution)/shard_map/all_to_all | solution.py:40
  257.6 9.3 %all-to-all-done.1 = f32[8,128,128]{2,1,0:T(8,128)S(1)} async-done(((f32[8,128,128]{2,1,0:T(8,128)}), f32[8,128,128]{2,1,0:T(8,128)S(1)}, u32[]{:S(2)}, u32[]{:S(2)}) %all-to-all-start.1) | async-done | bytes 524320 | tf_op jit(solution)/shard_map/all_to_all | solution.py:40
  267.7 0.3 concatenate.31
  268.2 120.2 %all_to_all.31 = f32[32,4,2049]{2,1,0:T(4,128)S(1)} all-to-all(f32[32,4,2049]{2,1,0:T(4,128)S(1)} %pad_maximum_fusion), channel_id=1, replica_groups=mesh['grp'=2,'kv'=32,'tp'=8] {'kv'}, dimensions={0} | all-to-all | bytes 2098176 | tf_op jit(solution)/shard_map/all_to_all | solution.py:23
  389.1 64.8 %all_to_all.32 = bf16[32,4,2048]{2,1,0:T(4,128)(2,1)S(1)} all-to-all(bf16[32,4,2048]{2,1,0:T(4,128)(2,1)S(1)} %broadcast_in_dim.10), channel_id=1, replica_groups=mesh['grp'=2,'kv'=32,'tp'=8] {'kv'}, dimensions={0} | all-to-all | bytes 1048576 | tf_op jit(solution)/shard_map/all_to_all | solution.py:40
  454.3 16.5 %all_to_all.33 = f32[8,128,128]{2,1,0:T(8,128)S(1)} all-to-all(f32[8,128,128]{2,1,0:T(8,128)S(1)} %broadcast_in_dim.11), channel_id=1, replica_groups=mesh['grp'=2,'kv'=32,'tp'=8] {'tp'}, dimensions={0} | all-to-all | bytes 1048576 | tf_op jit(solution)/shard_map/all_to_all | solution.py:40
  470.8 0.6 fusion.5
  (78 shorter events, 4.4 us)
Async XLA Ops:
  0.6 266.7 %copy-start = (bf16[128,2048]{1,0:T(8,128)(2,1)S(1)}, bf16[128,2048]{1,0:T(8,128)(2,1)}, u32[]{:S(2)}) copy-start(bf16[128,2048]{1,0:T(8,128)(2,1)} %param.38) | copy-start | bytes 1572868
  0.6 5.8 %copy-start.2 = (bf16[128,128]{1,0:T(8,128)(2,1)S(1)}, bf16[128,128]{1,0:T(8,128)(2,1)}, u32[]{:S(2)}) copy-start(bf16[128,128]{1,0:T(8,128)(2,1)} %param.20) | copy-start | bytes 98308
  0.7 5.8 %copy-start.6 = (bf16[128,512]{1,0:T(8,128)(2,1)S(1)}, bf16[128,512]{1,0:T(8,128)(2,1)}, u32[]{:S(2)}) copy-start(bf16[128,512]{1,0:T(8,128)(2,1)} %param.26) | copy-start | bytes 393220
  6.7 47.7 %copy-start.11 = (bf16[512]{0:T(512)(128)(2,1)S(1)}, bf16[512]{0:T(512)(128)(2,1)}, u32[]{:S(2)}) copy-start(bf16[512]{0:T(512)(128)(2,1)} %param.35) | copy-start | bytes 3076
  6.7 49.7 %copy-start.13 = (s32[4]{0:T(128)S(1)}, s32[4]{0:T(128)}, u32[]{:S(2)}) copy-start(s32[4]{0:T(128)} %param.21) | copy-start | bytes 52
  6.7 49.7 %copy-start.14 = (f32[8]{0:T(128)S(1)}, f32[8]{0:T(128)}, u32[]{:S(2)}) copy-start(f32[8]{0:T(128)} %param.32) | copy-start | bytes 100
  6.7 49.7 %copy-start.10 = (bf16[4,2,128]{2,1,0:T(2,128)(2,1)S(1)}, bf16[4,2,128]{2,1,0:T(2,128)(2,1)}, u32[]{:S(2)}) copy-start(bf16[4,2,128]{2,1,0:T(2,128)(2,1)} %param.34) | copy-start | bytes 6148
  6.7 49.7 %copy-start.7 = (bf16[4,512]{1,0:T(4,128)(2,1)S(1)}, bf16[4,512]{1,0:T(4,128)(2,1)}, u32[]{:S(2)}) copy-start(bf16[4,512]{1,0:T(4,128)(2,1)} %param.33) | copy-start | bytes 12292
  7.9 48.5 %copy-start.9 = (bf16[4,3,2,128]{3,2,1,0:T(2,128)(2,1)S(1)}, bf16[4,3,2,128]{3,2,1,0:T(2,128)(2,1)}, u32[]{:S(2)}) copy-start(bf16[4,3,2,128]{3,2,1,0:T(2,128)(2,1)} %param.23) | copy-start | bytes 18436
  7.9 48.6 %copy-start.8 = (bf16[4,3,512]{2,0,1:T(4,128)(2,1)S(1)}, bf16[4,3,512]{2,0,1:T(4,128)(2,1)}, u32[]{:S(2)}) copy-start(bf16[4,3,512]{2,0,1:T(4,128)(2,1)} %param.22) | copy-start | bytes 36868
  8.0 128.2 %copy-start.12 = (f32[8]{0:T(128)S(1)}, f32[8]{0:T(128)}, u32[]{:S(2)}) copy-start(f32[8]{0:T(128)} %param.31) | copy-start | bytes 100
  8.0 128.4 %copy-start.3 = (f32[4,8,64,128]{3,2,1,0:T(8,128)S(1)}, f32[4,8,64,128]{3,2,1,0:T(8,128)}, u32[]{:S(2)}) copy-start(f32[4,8,64,128]{3,2,1,0:T(8,128)} %param.24) | copy-start | bytes 3145732
  8.0 127.6 %all-to-all-start = ((f32[32,4,1289]{2,1,0:T(4,128)}), f32[32,4,1289]{2,1,0:T(4,128)S(1)}, u32[]{:S(2)}, u32[]{:S(2)}) async-start(f32[32,4,1289]{2,1,0:T(4,128)} %concatenate.30), calls=%async_computation | async-start | bytes 1441792 | tf_op jit(solution)/shard_map/all_to_all | solution.py:23
  136.8 102.2 %copy-start.1 = (f32[4,8,64,128]{3,2,1,0:T(8,128)}, f32[4,8,64,128]{3,2,1,0:T(8,128)S(1)}, u32[]{:S(2)}) copy-start(f32[4,8,64,128]{3,2,1,0:T(8,128)S(1)} %multiply_add_fusion) | copy-start | bytes 3145732
  136.8 101.2 %copy-start.5 = (bf16[512,128]{1,0:T(8,128)(2,1)S(1)}, bf16[512,128]{1,0:T(8,128)(2,1)}, u32[]{:S(2)}) copy-start(bf16[512,128]{1,0:T(8,128)(2,1)} %param.36) | copy-start | bytes 393220
  179.1 59.1 %all-to-all-start.2 = ((f32[8,1,128]{2,1,0:T(1,128)}), f32[8,1,128]{2,1,0:T(1,128)S(1)}, u32[]{:S(2)}, u32[]{:S(2)}) async-start(f32[8,1,128]{2,1,0:T(1,128)} %broadcast_in_dim.9), calls=%async_computation.2 | async-start | bytes 8192 | tf_op jit(solution)/shard_map/all_to_all | solution.py:40
  237.9 19.6 %copy-start.15 = (bf16[128]{0:T(256)(128)(2,1)S(1)}, bf16[128]{0:T(256)(128)(2,1)}, u32[]{:S(2)}) copy-start(bf16[128]{0:T(256)(128)(2,1)} %param.37) | copy-start | bytes 772
  239.0 27.9 %all-to-all-start.1 = ((f32[8,128,128]{2,1,0:T(8,128)}), f32[8,128,128]{2,1,0:T(8,128)S(1)}, u32[]{:S(2)}, u32[]{:S(2)}) async-start(f32[8,128,128]{2,1,0:T(8,128)} %broadcast_in_dim.8), calls=%async_computation.1 | async-start | bytes 1048576 | tf_op jit(solution)/shard_map/all_to_all | solution.py:40
  389.0 64.9 %copy-start.4 = (bf16[2048,128]{1,0:T(8,128)(2,1)S(1)}, bf16[2048,128]{1,0:T(8,128)(2,1)}, u32[]{:S(2)}) copy-start(bf16[2048,128]{1,0:T(8,128)(2,1)} %param.39) | copy-start | bytes 1572868
where the time goes:
time: 472 us; the launch traced here: 471 us
  blocking collectives  281 us (60%)
  waiting for transfers between devices  88.3 us (19%)
  starting transfers between devices  83.6 us (18%)
  matrix products  6.45 us (1%)
  local copies, waits for them, and re-layouts  5.78 us (1%)
    all_to_all x1, blocking collectives, summed_on_arrival(): lax.all_to_all(parts, axis, split_axis=0, concat_axis=0, tiled=True)  120 us
    all_to_all x2, blocking collectives, from_everyone(): return lax.all_to_all(copies, axis, split_axis=0, concat_axis=0, tiled=True)  81.3 us
    all_to_all x1, waiting for transfers between devices, summed_on_arrival(): lax.all_to_all(parts, axis, split_axis=0, concat_axis=0, tiled=True)  79 us
    all_to_all x1, starting transfers between devices, summed_on_arrival(): lax.all_to_all(parts, axis, split_axis=0, concat_axis=0, tiled=True)  46.4 us
    all_gather x1, blocking collectives, per_device(): lax.all_gather(gated_low, 'kv', axis=0, tiled=True)  40.2 us
    unnamed x1, blocking collectives  39.4 us
    all_to_all x2, starting transfers between devices, from_everyone(): return lax.all_to_all(copies, axis, split_axis=0, concat_axis=0, tiled=True)  37.2 us
  transfers between devices with their start and end apart: 3, of which 2 were waited for; matrix products, arithmetic and copies ran while one was open for 0% of the time, Pallas kernels for 0%

commit v1 on v0

v1 whole, which is shorter than its diff:
```python
import jax
import jax.numpy as jnp
from jax import lax
from jax.sharding import Mesh, PartitionSpec as P

HEAD_DIM = 64
STATE = 128
CONV_WIDTH = 4
LANES = 128
NEAR = 4

epsilon = 1e-06
f32, bf16 = jnp.float32, jnp.bfloat16


def scattered_sum(rows, along):
    size = lax.axis_size(along)
    parts = rows.reshape(size, -1, rows.shape[1])
    return lax.all_to_all(parts, along, 0, 0, tiled=True).astype(f32).sum(axis=0)


def from_everyone(shard, along):
    copies = jnp.broadcast_to(shard, (lax.axis_size(along), *shard.shape))
    return lax.all_to_all(copies, along, 0, 0, tiled=True)


def hi_lo(column):
    hi = column.astype(bf16)
    lo = (column - hi.astype(f32)).astype(bf16)
    lane = lax.broadcasted_iota(jnp.int32, (column.shape[0], LANES), 1)
    return jnp.where(lane == 0, hi, jnp.where(lane == 1, lo, jnp.zeros((), bf16)))


def causal_conv(state_rows, newest, conv_weights):
    extended = jnp.concatenate([state_rows, newest[:, None]], axis=1)
    conv_sum = extended[:, 0] * conv_weights[0].astype(f32)
    for offset in range(1, conv_weights.shape[0]):
        conv_sum = conv_sum + extended[:, offset] * conv_weights[offset].astype(f32)
    return jax.nn.silu(conv_sum)


def product(left, right, out=f32):
    return jnp.dot(left, right, preferred_element_type=out)


def per_device(
    tokens,
    lengths,
    conv_state_x,
    conv_state_bc,
    ssm_state,
    norm_gain,
    w_gate,
    w_value,
    w_key,
    w_query,
    w_step,
    step_bias,
    decay_log,
    conv_x,
    conv_bc,
    inner_gain,
    w_out,
    mlp_gain,
    w_up,
    w_down,
):
    far, near = lax.axis_size("far"), lax.axis_size("near")
    kv = ("far", "near")
    head_count = w_step.shape[1]
    group_count = w_key.shape[1] // STATE
    per_group = head_count // group_count
    batch, width = tokens.shape
    model = width * far * near
    inner = w_gate.shape[1] * lax.axis_size("tp")
    seqs = batch // (far * near)

    ordered = tokens.reshape(far, near, seqs, width).swapaxes(0, 1).reshape(batch, width)
    wide = ordered.astype(f32)
    scaled = (wide * norm_gain.astype(f32)).astype(bf16)
    partial = jnp.concatenate(
        [
            product(scaled, w_gate, bf16),
            product(scaled, w_value, bf16),
            product(scaled, w_key, bf16),
            product(scaled, w_query, bf16),
            product(scaled, w_step, bf16),
            hi_lo(jnp.sum(wide * wide, axis=1, keepdims=True))[:, : LANES - head_count],
        ],
        axis=1,
    )
    mine = scattered_sum(scattered_sum(partial, "near").astype(bf16), "far")
    cuts, at = [], 0
    for size in (w_gate.shape[1], w_value.shape[1], w_key.shape[1], w_query.shape[1], head_count):
        cuts.append(mine[:, at : at + size])
        at += size
    gate_raw, value_raw, key_raw, query_raw, step_raw = cuts
    squares = jnp.sum(mine[:, at:], axis=1, keepdims=True)
    inverse = lax.rsqrt(squares / model + epsilon)

    row_live = (
        jnp.arange(CONV_WIDTH - 1, dtype=jnp.int32)[None, :] >= CONV_WIDTH - 1 - lengths[:, None]
    ).astype(f32)
    live_x = conv_state_x.astype(f32) * row_live[:, :, None]
    live_bc = conv_state_bc.astype(f32) * row_live[:, :, None, None]
    mixed_values = causal_conv(live_x, value_raw * inverse, conv_x).reshape(
        seqs, head_count, HEAD_DIM
    )
    key_query = causal_conv(
        live_bc, jnp.stack([key_raw * inverse, query_raw * inverse], axis=1), conv_bc
    )
    key_heads = jnp.repeat(key_query[:, 0].reshape(seqs, group_count, STATE), per_group, axis=1)
    query_heads = jnp.repeat(key_query[:, 1].reshape(seqs, group_count, STATE), per_group, axis=1)
    step_size = jax.nn.softplus(step_raw * inverse + step_bias)
    rate_now = -jnp.exp(decay_log) * step_size
    next_state = (
        ssm_state * jnp.exp(rate_now)[:, :, None, None]
        + (step_size[:, :, None] * mixed_values)[:, :, :, None] * key_heads[:, :, None, :]
    )
    mixer_y = jnp.sum(next_state * query_heads[:, :, None, :], axis=3).reshape(
        seqs, head_count * HEAD_DIM
    )
    gated_rows = mixer_y * jax.nn.silu(gate_raw * inverse)
    gated_low = (gated_rows * inner_gain.astype(f32)).astype(bf16)

    all_low = from_everyone(gated_low, kv).reshape(batch, -1)
    ungained = all_low.astype(f32) / inner_gain.astype(f32)
    gated_squares = jnp.sum(ungained * ungained, axis=1)
    high = gated_squares.astype(bf16)
    low = (gated_squares - high.astype(f32)).astype(bf16)
    out_part = product(all_low, w_out, bf16)
    shared = from_everyone(jnp.concatenate([out_part, high[None], low[None]], axis=0), "tp")
    shared = shared.astype(f32).sum(axis=0)
    out_sum, gated_total = shared[:batch], shared[batch] + shared[batch + 1]
    residual = (
        tokens.astype(f32) + out_sum * lax.rsqrt(gated_total / inner + epsilon)[:, None]
    ).astype(bf16)

    residual_wide = residual.astype(f32)
    hidden_low = (residual_wide * mlp_gain.astype(f32)).astype(bf16)
    row_squares = jnp.sum(residual_wide * residual_wide, axis=1, keepdims=True)
    up_part = jnp.concatenate([product(hidden_low, w_up, bf16), hi_lo(row_squares)], axis=1)
    up_mine = scattered_sum(scattered_sum(up_part, "near").astype(bf16), "far")
    up_share, square_share = up_mine[:, :-LANES], jnp.sum(up_mine[:, -LANES:], axis=1, keepdims=True)
    active = jnp.square(
        jax.nn.relu(up_share * lax.rsqrt(square_share / model + epsilon))
    ).astype(bf16)
    active = from_everyone(active, "far").reshape(-1, active.shape[1])
    active = from_everyone(active, "near").reshape(batch, -1)
    down_sum = from_everyone(product(active, w_down, bf16), "tp").astype(f32).sum(axis=0)
    return ((residual_wide + down_sum).astype(bf16), next_state)


def solution(mesh):
    kv = mesh.shape["kv"]
    near = NEAR if kv % NEAR == 0 else 1
    names = ("grp", "far", "near", "tp")
    split = Mesh(mesh.devices.reshape(mesh.shape["grp"], kv // near, near, mesh.shape["tp"]), names)
    kv = ("far", "near")
    seq = ("grp", "far", "near")
    return jax.shard_map(
        per_device,
        mesh=split,
        in_specs=(
            P("grp", kv),
            P(seq),
            P(seq, None, "tp"),
            P(seq, None, None, "tp"),
            P(seq, "tp", None, None),
            P(kv),
            P(kv, "tp"),
            P(kv, "tp"),
            P(kv, "tp"),
            P(kv, "tp"),
            P(kv, "tp"),
            P("tp"),
            P("tp"),
            P(None, "tp"),
            P(None, None, "tp"),
            P("tp"),
            P("tp", kv),
            P(kv),
            P(kv, "tp"),
            P("tp", kv),
        ),
        out_specs=(P("grp", kv), P(seq, "tp", None, None)),
        check_vma=False,
    )
```

time: 472 us -> 257 us (0.54)
  blocking collectives: 281 us -> 140 us
  waiting for transfers between devices: 88.3 us -> 36 us
  starting transfers between devices: 83.6 us -> 63.5 us
    all_to_all x3 -> x6, blocking collectives: 201 us -> 140 us  [the longest x4 97.1 us: from_everyone(): return lax.all_to_all(copies, along, 0, 0, tiled=True)]
    all_to_all x3, waiting for transfers between devices: 88.3 us -> 36 us  [the longest x2 29.4 us: scattered_sum(): lax.all_to_all(parts, along, 0, 0, tiled=True).astype(f32).sum(axis=0)]
    all_gather x1 -> x0, blocking collectives: 40.2 us -> none  [per_device(): lax.all_gather(gated_low, 'kv', axis=0, tiled=True)]
    unnamed x1 -> x0, blocking collectives: 39.4 us -> none
    all_to_all x3, starting transfers between devices: 83.6 us -> 63.5 us  [the longest x2 53.4 us: scattered_sum(): lax.all_to_all(parts, along, 0, 0, tiled=True).astype(f32).sum(axis=0)]
  transfers between devices with their start and end apart: 3 -> 3, of which waited for: 2 -> 3; matrix products, arithmetic and copies ran while one was open for 0% -> 0% of each run, Pallas kernels for 0% -> 0%
where the time goes in v1:
time: 257 us; the launch traced here: 256 us
  blocking collectives  140 us (54%)
  starting transfers between devices  63.5 us (25%)
  waiting for transfers between devices  36 us (14%)
  other arithmetic  5.66 us (2%)
  matrix products  5.5 us (2%)
  local copies, waits for them, and re-layouts  3.95 us (2%)
    all_to_all x4, blocking collectives, from_everyone(): return lax.all_to_all(copies, along, 0, 0, tiled=True)  97.1 us
    all_to_all x2, starting transfers between devices, scattered_sum(): lax.all_to_all(parts, along, 0, 0, tiled=True).astype(f32).sum(axis=0)  53.4 us
    all_to_all x2, blocking collectives, scattered_sum(): lax.all_to_all(parts, along, 0, 0, tiled=True).astype(f32).sum(axis=0)  43.3 us
    all_to_all x2, waiting for transfers between devices, scattered_sum(): lax.all_to_all(parts, along, 0, 0, tiled=True).astype(f32).sum(axis=0)  29.4 us
    all_to_all x1, starting transfers between devices, from_everyone(): return lax.all_to_all(copies, along, 0, 0, tiled=True)  10.1 us
    all_to_all x1, waiting for transfers between devices, from_everyone(): return lax.all_to_all(copies, along, 0, 0, tiled=True)  6.62 us
    dot_general x8, matrix products, product(): return jnp.dot(left, right, preferred_element_type=out)  5.5 us
  transfers between devices with their start and end apart: 3, of which 3 were waited for; matrix products, arithmetic and copies ran while one was open for 0% of the time, Pallas kernels for 0%

profile of v1, /device:TPU:33, one launch (start us, length us, event | category | flops | bytes accessed | tf_op | source)
XLA Modules:
  0.0 256.1 jit_solution(15360752176402715215)
XLA Ops:
  0.7 0.7 convert_element_type.195
  1.4 0.9 multiply_reduce_fusion.2
  2.5 0.8 copy.78
  3.3 0.8 fusion.37
  4.1 0.9 fusion.36
  5.0 0.9 fusion.35
  5.9 1.1 fusion.34
  7.0 1.1 fusion.33
  8.2 0.8 concatenate.9
  9.1 9.2 %all-to-all-start = ((bf16[4,32,1408]{2,1,0:T(8,128)(2,1)}), bf16[4,32,1408]{2,1,0:T(8,128)(2,1)S(1)}, u32[]{:S(2)}, u32[]{:S(2)}) async-start(bf16[4,32,1408]{2,1,0:T(8,128)(2,1)} %bitcast.4), calls=%async_computation | async-start | bytes 720896 | tf_op jit(solution)/shard_map/all_to_all | solution.py:19
  18.3 6.3 %all-to-all-done = bf16[4,32,1408]{2,1,0:T(8,128)(2,1)S(1)} async-done(((bf16[4,32,1408]{2,1,0:T(8,128)(2,1)}), bf16[4,32,1408]{2,1,0:T(8,128)(2,1)S(1)}, u32[]{:S(2)}, u32[]{:S(2)}) %all-to-all-start) | async-done | bytes 360480 | tf_op jit(solution)/shard_map/all_to_all | solution.py:19
  24.7 0.7 reshape.201
  25.4 44.3 %all-to-all-start.1 = ((bf16[8,4,1408]{2,1,0:T(4,128)(2,1)}), bf16[8,4,1408]{2,1,0:T(4,128)(2,1)S(1)}, u32[]{:S(2)}, u32[]{:S(2)}) async-start(bf16[8,4,1408]{2,1,0:T(4,128)(2,1)} %reshape.201), calls=%async_computation.1 | async-start | bytes 180224 | tf_op jit(solution)/shard_map/all_to_all | solution.py:19
  69.9 23.0 %all-to-all-done.1 = bf16[8,4,1408]{2,1,0:T(4,128)(2,1)S(1)} async-done(((bf16[8,4,1408]{2,1,0:T(4,128)(2,1)}), bf16[8,4,1408]{2,1,0:T(4,128)(2,1)S(1)}, u32[]{:S(2)}, u32[]{:S(2)}) %all-to-all-start.1) | async-done | bytes 90144 | tf_op jit(solution)/shard_map/all_to_all | solution.py:19
  93.6 1.4 multiply_reduce_fusion
  95.2 30.8 %all_to_all.45 = bf16[32,4,512]{2,1,0:T(4,128)(2,1)S(1)} all-to-all(bf16[32,4,512]{2,1,0:T(4,128)(2,1)S(1)} %broadcast_in_dim.44), channel_id=1, replica_groups=mesh['grp'=2,'far'=8,'near'=4,'tp'=8] {'far','near'}, dimensions={0} | all-to-all | bytes 262144 | tf_op jit(solution)/shard_map/all_to_all | solution.py:24
  126.6 0.7 broadcast_in_dim.45
  127.3 10.1 %all-to-all-start.3 = ((bf16[8,130,128]{2,1,0:T(8,128)(2,1)}), bf16[8,130,128]{2,1,0:T(8,128)(2,1)S(1)}, u32[]{:S(2)}, u32[]{:S(2)}) async-start(bf16[8,130,128]{2,1,0:T(8,128)(2,1)} %broadcast_in_dim.45), calls=%async_computation.3 | async-start | bytes 557056 | tf_op jit(solution)/shard_map/all_to_all | solution.py:24
  137.4 6.6 %all-to-all-done.3 = bf16[8,130,128]{2,1,0:T(8,128)(2,1)S(1)} async-done(((bf16[8,130,128]{2,1,0:T(8,128)(2,1)}), bf16[8,130,128]{2,1,0:T(8,128)(2,1)S(1)}, u32[]{:S(2)}, u32[]{:S(2)}) %all-to-all-start.3) | async-done | bytes 266272 | tf_op jit(solution)/shard_map/all_to_all | solution.py:24
  144.9 17.0 %all_to_all.46 = bf16[4,32,2176]{2,1,0:T(8,128)(2,1)S(1)} all-to-all(bf16[4,32,2176]{2,1,0:T(8,128)(2,1)S(1)} %bitcast.108), channel_id=1, replica_groups=mesh['grp'=2,'far'=8,'near'=4,'tp'=8] {'near'}, dimensions={0} | all-to-all | bytes 1114112 | tf_op jit(solution)/shard_map/all_to_all | solution.py:19
  162.0 26.4 %all_to_all.47 = bf16[8,4,2176]{2,1,0:T(4,128)(2,1)S(1)} all-to-all(bf16[8,4,2176]{2,1,0:T(4,128)(2,1)S(1)} %reshape.206), channel_id=1, replica_groups=mesh['grp'=2,'far'=8,'near'=4,'tp'=8] {'far'}, dimensions={0} | all-to-all | bytes 278528 | tf_op jit(solution)/shard_map/all_to_all | solution.py:19
  188.7 35.5 %all_to_all.48 = bf16[8,4,2048]{2,1,0:T(4,128)(2,1)S(1)} all-to-all(bf16[8,4,2048]{2,1,0:T(4,128)(2,1)S(1)} %broadcast_in_dim.48), channel_id=1, replica_groups=mesh['grp'=2,'far'=8,'near'=4,'tp'=8] {'far'}, dimensions={0} | all-to-all | bytes 262144 | tf_op jit(solution)/shard_map/all_to_all | solution.py:24
  224.3 19.9 %all_to_all.49 = bf16[4,32,2048]{2,1,0:T(8,128)(2,1)S(1)} all-to-all(bf16[4,32,2048]{2,1,0:T(8,128)(2,1)S(1)} %broadcast_in_dim.84), channel_id=1, replica_groups=mesh['grp'=2,'far'=8,'near'=4,'tp'=8] {'near'}, dimensions={0} | all-to-all | bytes 1048576 | tf_op jit(solution)/shard_map/all_to_all | solution.py:24
  244.6 10.9 %all_to_all.50 = bf16[8,128,128]{2,1,0:T(8,128)(2,1)S(1)} all-to-all(bf16[8,128,128]{2,1,0:T(8,128)(2,1)S(1)} %broadcast_in_dim.85), channel_id=1, replica_groups=mesh['grp'=2,'far'=8,'near'=4,'tp'=8] {'tp'}, dimensions={0} | all-to-all | bytes 524288 | tf_op jit(solution)/shard_map/all_to_all | solution.py:24
  (85 shorter events, 4.4 us)
Async XLA Ops:
  0.6 143.9 %copy-start = (bf16[128,2048]{1,0:T(8,128)(2,1)S(1)}, bf16[128,2048]{1,0:T(8,128)(2,1)}, u32[]{:S(2)}) copy-start(bf16[128,2048]{1,0:T(8,128)(2,1)} %param.38) | copy-start | bytes 1572868
  5.9 12.4 %copy-start.9 = (bf16[512]{0:T(512)(128)(2,1)S(1)}, bf16[512]{0:T(512)(128)(2,1)}, u32[]{:S(2)}) copy-start(bf16[512]{0:T(512)(128)(2,1)} %param.35) | copy-start | bytes 3076
  5.9 12.4 %copy-start.11 = (s32[4]{0:T(128)S(1)}, s32[4]{0:T(128)}, u32[]{:S(2)}) copy-start(s32[4]{0:T(128)} %param.21) | copy-start | bytes 52
  5.9 12.4 %copy-start.8 = (bf16[4,2,128]{2,1,0:T(2,128)(2,1)S(1)}, bf16[4,2,128]{2,1,0:T(2,128)(2,1)}, u32[]{:S(2)}) copy-start(bf16[4,2,128]{2,1,0:T(2,128)(2,1)} %param.34) | copy-start | bytes 6148
  5.9 12.4 %copy-start.5 = (bf16[4,512]{1,0:T(4,128)(2,1)S(1)}, bf16[4,512]{1,0:T(4,128)(2,1)}, u32[]{:S(2)}) copy-start(bf16[4,512]{1,0:T(4,128)(2,1)} %param.33) | copy-start | bytes 12292
  8.2 61.5 %copy-start.12 = (f32[8]{0:T(128)S(1)}, f32[8]{0:T(128)}, u32[]{:S(2)}) copy-start(f32[8]{0:T(128)} %param.32) | copy-start | bytes 100
  8.2 61.5 %copy-start.7 = (bf16[4,3,2,128]{3,2,1,0:T(2,128)(2,1)S(1)}, bf16[4,3,2,128]{3,2,1,0:T(2,128)(2,1)}, u32[]{:S(2)}) copy-start(bf16[4,3,2,128]{3,2,1,0:T(2,128)(2,1)} %param.23) | copy-start | bytes 18436
  8.2 61.5 %copy-start.6 = (bf16[4,3,512]{2,0,1:T(4,128)(2,1)S(1)}, bf16[4,3,512]{2,0,1:T(4,128)(2,1)}, u32[]{:S(2)}) copy-start(bf16[4,3,512]{2,0,1:T(4,128)(2,1)} %param.22) | copy-start | bytes 36868
  9.1 84.4 %copy-start.10 = (f32[8]{0:T(128)S(1)}, f32[8]{0:T(128)}, u32[]{:S(2)}) copy-start(f32[8]{0:T(128)} %param.31) | copy-start | bytes 100
  9.1 84.5 %copy-start.1 = (f32[4,8,64,128]{3,2,1,0:T(8,128)S(1)}, f32[4,8,64,128]{3,2,1,0:T(8,128)}, u32[]{:S(2)}) copy-start(f32[4,8,64,128]{3,2,1,0:T(8,128)} %param.24) | copy-start | bytes 3145732
  9.1 15.6 %all-to-all-start = ((bf16[4,32,1408]{2,1,0:T(8,128)(2,1)}), bf16[4,32,1408]{2,1,0:T(8,128)(2,1)S(1)}, u32[]{:S(2)}, u32[]{:S(2)}) async-start(bf16[4,32,1408]{2,1,0:T(8,128)(2,1)} %bitcast.4), calls=%async_computation | async-start | bytes 720896 | tf_op jit(solution)/shard_map/all_to_all | solution.py:19
  25.4 67.5 %all-to-all-start.1 = ((bf16[8,4,1408]{2,1,0:T(4,128)(2,1)}), bf16[8,4,1408]{2,1,0:T(4,128)(2,1)S(1)}, u32[]{:S(2)}, u32[]{:S(2)}) async-start(bf16[8,4,1408]{2,1,0:T(4,128)(2,1)} %reshape.201), calls=%async_computation.1 | async-start | bytes 180224 | tf_op jit(solution)/shard_map/all_to_all | solution.py:19
  93.6 32.8 %copy-start.4 = (bf16[512,128]{1,0:T(8,128)(2,1)S(1)}, bf16[512,128]{1,0:T(8,128)(2,1)}, u32[]{:S(2)}) copy-start(bf16[512,128]{1,0:T(8,128)(2,1)} %param.36) | copy-start | bytes 393220
  95.0 42.4 %copy-start.13 = (bf16[128]{0:T(256)(128)(2,1)S(1)}, bf16[128]{0:T(256)(128)(2,1)}, u32[]{:S(2)}) copy-start(bf16[128]{0:T(256)(128)(2,1)} %param.37) | copy-start | bytes 772
  126.0 18.2 %copy-start.3 = (bf16[128,128]{1,0:T(8,128)(2,1)S(1)}, bf16[128,128]{1,0:T(8,128)(2,1)}, u32[]{:S(2)}) copy-start(bf16[128,128]{1,0:T(8,128)(2,1)} %param.20) | copy-start | bytes 98308
  127.3 16.7 %all-to-all-start.3 = ((bf16[8,130,128]{2,1,0:T(8,128)(2,1)}), bf16[8,130,128]{2,1,0:T(8,128)(2,1)S(1)}, u32[]{:S(2)}, u32[]{:S(2)}) async-start(bf16[8,130,128]{2,1,0:T(8,128)(2,1)} %broadcast_in_dim.45), calls=%async_computation.3 | async-start | bytes 557056 | tf_op jit(solution)/shard_map/all_to_all | solution.py:24
  224.2 20.0 %copy-start.2 = (bf16[2048,128]{1,0:T(8,128)(2,1)S(1)}, bf16[2048,128]{1,0:T(8,128)(2,1)}, u32[]{:S(2)}) copy-start(bf16[2048,128]{1,0:T(8,128)(2,1)} %param.39) | copy-start | bytes 1572868

commit v2 on v1

--- a/solution.py
+++ b/solution.py
@@ -1,6 +1,9 @@
+import functools
+
 import jax
 import jax.numpy as jnp
 from jax import lax
+from jax.experimental import pallas as pl
 from jax.sharding import Mesh, PartitionSpec as P
 
 HEAD_DIM = 64
@@ -29,6 +32,54 @@
     lo = (column - hi.astype(f32)).astype(bf16)
     lane = lax.broadcasted_iota(jnp.int32, (column.shape[0], LANES), 1)
     return jnp.where(lane == 0, hi, jnp.where(lane == 1, lo, jnp.zeros((), bf16)))
+
+
+def project_kernel(
+    far, near, seqs, tokens_ref, gain_ref, gate_ref, value_ref, key_ref, query_ref, step_ref, sent_ref
+):
+    batch, width = tokens_ref.shape
+    to = lax.broadcasted_iota(jnp.int32, (batch, batch), 0)
+    at = lax.broadcasted_iota(jnp.int32, (batch, batch), 1)
+    group = to // (far * seqs)
+    rest = to - group * (far * seqs)
+    block = rest // seqs
+    source = (block * near + group) * seqs + rest - block * seqs
+    order = jnp.where(at == source, 1.0, 0.0).astype(bf16)
+    wide = product(order, tokens_ref[...])
+    scaled = (wide * gain_ref[...].astype(f32)).astype(bf16)
+    column = 0
+    for weight in (gate_ref, value_ref, key_ref, query_ref):
+        size = weight.shape[1]
+        sent_ref[:, column : column + size] = product(scaled, weight[...]).astype(bf16)
+        column += size
+    heads = step_ref.shape[0]
+    steps = jnp.concatenate(
+        [step_ref[...].astype(f32), jnp.zeros((LANES - heads, width), f32)], axis=0
+    ).astype(bf16)
+    steps = lax.dot_general(
+        scaled, steps, (((1,), (1,)), ((), ())), preferred_element_type=f32
+    )
+    squares = jnp.sum(wide * wide, axis=1, keepdims=True)
+    high = squares.astype(bf16).astype(f32)
+    lane = lax.broadcasted_iota(jnp.int32, (batch, LANES), 1)
+    steps = jnp.where(lane == heads, high, jnp.where(lane == heads + 1, squares - high, steps))
+    sent_ref[:, column : column + LANES] = steps.astype(bf16)
+    sent_ref[:, column + LANES :] = wide.astype(bf16)
+
+
+def project(tokens, norm_gain, w_gate, w_value, w_key, w_query, w_step, far, near):
+    batch, width = tokens.shape
+    columns = sum(w.shape[1] for w in (w_gate, w_value, w_key, w_query)) + LANES + width
+    return pl.pallas_call(
+        functools.partial(project_kernel, far, near, batch // (far * near)),
+        out_shape=jax.ShapeDtypeStruct((batch, columns), bf16),
+        cost_estimate=pl.CostEstimate(
+            flops=2 * batch * width * columns,
+            bytes_accessed=2 * columns * (batch + width),
+            transcendentals=0,
+        ),
+        name="project",
+    )(tokens, norm_gain[None], w_gate, w_value, w_key, w_query, w_step.T)
 
 
 def causal_conv(state_rows, newest, conv_weights):
@@ -66,7 +117,6 @@
     w_down,
 ):
     far, near = lax.axis_size("far"), lax.axis_size("near")
-    kv = ("far", "near")
     head_count = w_step.shape[1]
     group_count = w_key.shape[1] // STATE
     per_group = head_count // group_count
@@ -75,21 +125,45 @@
     inner = w_gate.shape[1] * lax.axis_size("tp")
     seqs = batch // (far * near)
 
-    ordered = tokens.reshape(far, near, seqs, width).swapaxes(0, 1).reshape(batch, width)
-    wide = ordered.astype(f32)
-    scaled = (wide * norm_gain.astype(f32)).astype(bf16)
-    partial = jnp.concatenate(
+    sent = project(tokens, norm_gain, w_gate, w_value, w_key, w_query, w_step, far, near)
+    cols = sent.shape[1] - width
+    came = lax.all_to_all(sent.reshape(near, -1, cols + width), "near", 0, 0, tiled=True)
+    near_sum = came[:, :, :cols].astype(f32).sum(axis=0).astype(bf16)
+    near_tokens = came[:, :, cols:].swapaxes(0, 1).reshape(-1, near * width)
+    mine = scattered_sum(near_sum, "far")
+
+    hidden = w_up.shape[1] // near
+    blocks = hidden // width
+    extra = jnp.concatenate(
+        [jnp.broadcast_to(mlp_gain[None], (8, width)), near_sum[:8, :width]], axis=0
+    )
+    packed = jnp.concatenate(
         [
-            product(scaled, w_gate, bf16),
-            product(scaled, w_value, bf16),
-            product(scaled, w_key, bf16),
-            product(scaled, w_query, bf16),
-            product(scaled, w_step, bf16),
-            hi_lo(jnp.sum(wide * wide, axis=1, keepdims=True))[:, : LANES - head_count],
+            w_up.reshape(width, near, blocks, width).transpose(1, 2, 0, 3).reshape(near, -1, width),
+            w_down.reshape(near, -1, width),
+            jnp.broadcast_to(w_out[None], (near, *w_out.shape)),
+            jnp.broadcast_to(extra[None], (near, *extra.shape)),
         ],
         axis=1,
     )
-    mine = scattered_sum(scattered_sum(partial, "near").astype(bf16), "far")
+    here = lax.axis_index("near")
+    pieces = []
+    for step in range(near):
+        piece = lax.dynamic_index_in_dim(packed, here ^ step, keepdims=False)
+        if step:
+            with jax.named_scope("swap"):
+                piece = lax.ppermute(piece, "near", [(i, i ^ step) for i in range(near)])
+        pieces.append(piece)
+    pieces = jnp.stack(pieces)
+    swapped = jnp.stack(
+        [lax.dynamic_index_in_dim(pieces, here ^ i, keepdims=False) for i in range(near)]
+    )
+    own_up = swapped[:, :hidden].reshape(near, blocks, width, width)
+    own_up = own_up.transpose(0, 2, 1, 3).reshape(near * width, hidden)
+    own_down = swapped[:, hidden : 2 * hidden]
+    own_out = swapped[:, 2 * hidden : 2 * hidden + w_out.shape[0]]
+    near_gain = swapped[:, 2 * hidden + w_out.shape[0]].reshape(1, near * width)
+
     cuts, at = [], 0
     for size in (w_gate.shape[1], w_value.shape[1], w_key.shape[1], w_query.shape[1], head_count):
         cuts.append(mine[:, at : at + size])
@@ -123,32 +197,38 @@
     gated_rows = mixer_y * jax.nn.silu(gate_raw * inverse)
     gated_low = (gated_rows * inner_gain.astype(f32)).astype(bf16)
 
-    all_low = from_everyone(gated_low, kv).reshape(batch, -1)
+    all_low = from_everyone(gated_low, "far").reshape(far * seqs, -1)
     ungained = all_low.astype(f32) / inner_gain.astype(f32)
-    gated_squares = jnp.sum(ungained * ungained, axis=1)
-    high = gated_squares.astype(bf16)
-    low = (gated_squares - high.astype(f32)).astype(bf16)
-    out_part = product(all_low, w_out, bf16)
-    shared = from_everyone(jnp.concatenate([out_part, high[None], low[None]], axis=0), "tp")
+    gated_squares = hi_lo(jnp.sum(ungained * ungained, axis=1, keepdims=True))
+    out_part = [product(all_low, own_out[i], bf16) for i in range(near)]
+    shared = from_everyone(jnp.concatenate([*out_part, gated_squares], axis=1), "tp")
     shared = shared.astype(f32).sum(axis=0)
-    out_sum, gated_total = shared[:batch], shared[batch] + shared[batch + 1]
+    gated_total = jnp.sum(shared[:, near * width :], axis=1, keepdims=True)
     residual = (
-        tokens.astype(f32) + out_sum * lax.rsqrt(gated_total / inner + epsilon)[:, None]
+        near_tokens.astype(f32)
+        + shared[:, : near * width] * lax.rsqrt(gated_total / inner + epsilon)
     ).astype(bf16)
 
+    residual = from_everyone(residual, "near").reshape(batch, near * width)
     residual_wide = residual.astype(f32)
-    hidden_low = (residual_wide * mlp_gain.astype(f32)).astype(bf16)
+    hidden_low = (residual_wide * near_gain.astype(f32)).astype(bf16)
     row_squares = jnp.sum(residual_wide * residual_wide, axis=1, keepdims=True)
-    up_part = jnp.concatenate([product(hidden_low, w_up, bf16), hi_lo(row_squares)], axis=1)
-    up_mine = scattered_sum(scattered_sum(up_part, "near").astype(bf16), "far")
-    up_share, square_share = up_mine[:, :-LANES], jnp.sum(up_mine[:, -LANES:], axis=1, keepdims=True)
+    up_part = jnp.concatenate([product(hidden_low, own_up, bf16), hi_lo(row_squares)], axis=1)
+    up_mine = scattered_sum(up_part, "far")
+    up_share, square_share = up_mine[:, :hidden], jnp.sum(up_mine[:, hidden:], axis=1, keepdims=True)
     active = jnp.square(
         jax.nn.relu(up_share * lax.rsqrt(square_share / model + epsilon))
     ).astype(bf16)
-    active = from_everyone(active, "far").reshape(-1, active.shape[1])
-    active = from_everyone(active, "near").reshape(batch, -1)
-    down_sum = from_everyone(product(active, w_down, bf16), "tp").astype(f32).sum(axis=0)
-    return ((residual_wide + down_sum).astype(bf16), next_state)
+    active = from_everyone(active, "far").reshape(batch, hidden)
+    tp = lax.axis_size("tp")
+    down_part = jnp.stack([product(active, own_down[i], bf16) for i in range(near)])
+    down_part = down_part.reshape(near * tp, batch // tp, width)
+    down_sum = lax.all_to_all(down_part, ("near", "tp"), 0, 0, tiled=True).astype(f32).sum(axis=0)
+    own_rows = residual.reshape(tp, batch // tp, near, width).swapaxes(1, 2)
+    own_rows = own_rows[lax.axis_index("tp"), lax.axis_index("near")]
+    finished = (own_rows.astype(f32) + down_sum).astype(bf16)
+    finished = from_everyone(finished, "tp").reshape(near, far, seqs, width)
+    return (finished.swapaxes(0, 1).reshape(batch, width), next_state)
 
 
 def solution(mesh):

time: 257 us -> 245 us (0.953)
  blocking collectives: 140 us -> 55.9 us
  waiting for transfers between devices: 36 us -> 70.1 us
  starting transfers between devices: 63.5 us -> 97.2 us
  matrix products: 5.5 us -> 1.57 us
  other arithmetic: 5.66 us -> 8.83 us
  local copies, waits for them, and re-layouts: 3.95 us -> 6.8 us
    all_to_all x4 -> x2, blocking collectives: 97.1 us -> 23.6 us  [from_everyone(): return lax.all_to_all(copies, along, 0, 0, tiled=True)]
    all_to_all x1 -> x3, waiting for transfers between devices: 6.62 us -> 45 us  [from_everyone(): return lax.all_to_all(copies, along, 0, 0, tiled=True)]
    all_to_all x0 -> x2, starting transfers between devices: none -> 23.4 us  [the longest x1 14.4 us: per_device(): lax.all_to_all(down_part, ('near', 'tp'), 0, 0, tiled=True).astype(f32)]
    all_to_all x2 -> x1, waiting for transfers between devices: 29.4 us -> 11.5 us  [scattered_sum(): lax.all_to_all(parts, along, 0, 0, tiled=True).astype(f32).sum(axis=0)]
    all_to_all x0 -> x2, waiting for transfers between devices: none -> 12.2 us  [the longest x1 8.38 us: per_device(): lax.all_to_all(down_part, ('near', 'tp'), 0, 0, tiled=True).astype(f32)]
    all_to_all x2 -> x1, blocking collectives: 43.3 us -> 32.3 us  [scattered_sum(): lax.all_to_all(parts, along, 0, 0, tiled=True).astype(f32).sum(axis=0)]
    all_to_all x1 -> x3, starting transfers between devices: 10.1 us -> 20.4 us  [from_everyone(): return lax.all_to_all(copies, along, 0, 0, tiled=True)]
    all_to_all x2 -> x1, starting transfers between devices: 53.4 us -> 44 us  [scattered_sum(): lax.all_to_all(parts, along, 0, 0, tiled=True).astype(f32).sum(axis=0)]
  transfers between devices with their start and end apart: 3 -> 9, of which waited for: 3 -> 7; matrix products, arithmetic and copies ran while one was open for 0% -> 4% of each run, Pallas kernels for 0% -> 0%
where the time goes in v2:
time: 245 us; the launch traced here: 244 us
  starting transfers between devices  97.2 us (40%)
  waiting for transfers between devices  70.1 us (29%)
  blocking collectives  55.9 us (23%)
  other arithmetic  8.83 us (4%)
  local copies, waits for them, and re-layouts  6.8 us (3%)
    all_to_all x3, waiting for transfers between devices, from_everyone(): return lax.all_to_all(copies, along, 0, 0, tiled=True)  45 us
    all_to_all x1, starting transfers between devices, scattered_sum(): lax.all_to_all(parts, along, 0, 0, tiled=True).astype(f32).sum(axis=0)  44 us
    all_to_all x1, blocking collectives, scattered_sum(): lax.all_to_all(parts, along, 0, 0, tiled=True).astype(f32).sum(axis=0)  32.3 us
    all_to_all x2, blocking collectives, from_everyone(): return lax.all_to_all(copies, along, 0, 0, tiled=True)  23.6 us
    all_to_all x3, starting transfers between devices, from_everyone(): return lax.all_to_all(copies, along, 0, 0, tiled=True)  20.4 us
    all_to_all x1, starting transfers between devices, per_device(): lax.all_to_all(down_part, ('near', 'tp'), 0, 0, tiled=True).astype(f32)  14.4 us
    all_to_all x1, waiting for transfers between devices, scattered_sum(): lax.all_to_all(parts, along, 0, 0, tiled=True).astype(f32).sum(axis=0)  11.5 us
    ppermute x3, starting transfers between devices, per_device(): piece = lax.ppermute(piece, 'near', [(i, i ^ step) for i in range(near)])  9.35 us
  transfers between devices with their start and end apart: 9, of which 7 were waited for; matrix products, arithmetic and copies ran while one was open for 4% of the time, Pallas kernels for 0%

profile of v2, /device:TPU:33, one launch (start us, length us, event | category | flops | bytes accessed | tf_op | source)
XLA Modules:
  0.0 243.6 jit_solution(11121558793795635763)
XLA Ops:
  0.7 2.2 project.1
  2.9 9.0 %all-to-all-start = ((bf16[4,32,1536]{2,1,0:T(8,128)(2,1)}), bf16[4,32,1536]{2,1,0:T(8,128)(2,1)S(1)}, u32[]{:S(2)}, u32[]{:S(2)}) async-start(bf16[4,32,1536]{2,1,0:T(8,128)(2,1)} %bitcast.171), calls=%async_computation | async-start | bytes 786432 | tf_op jit(solution)/shard_map/all_to_all | solution.py:130
  14.1 0.8 slice_convert_fusion.3
  15.8 3.8 %all-to-all-done = bf16[4,32,1536]{2,1,0:T(8,128)(2,1)S(1)} async-done(((bf16[4,32,1536]{2,1,0:T(8,128)(2,1)}), bf16[4,32,1536]{2,1,0:T(8,128)(2,1)S(1)}, u32[]{:S(2)}, u32[]{:S(2)}) %all-to-all-start) | async-done | bytes 393248 | tf_op jit(solution)/shard_map/all_to_all | solution.py:130
  20.4 44.0 %all-to-all-start.1 = ((bf16[8,4,1408]{2,1,0:T(4,128)(2,1)}), bf16[8,4,1408]{2,1,0:T(4,128)(2,1)S(1)}, u32[]{:S(2)}, u32[]{:S(2)}) async-start(bf16[8,4,1408]{2,1,0:T(4,128)(2,1)} %reshape.201), calls=%async_computation.1 | async-start | bytes 180224 | tf_op jit(solution)/shard_map/all_to_all | solution.py:22
  65.2 1.1 constant_dynamic-slice_fusion.4
  66.3 1.9 collective-permute-start
  68.2 3.0 %collective-permute-start.1 = (bf16[1552,128]{1,0:T(8,128)(2,1)}, bf16[1552,128]{1,0:T(8,128)(2,1)S(1)}, u32[]{:S(2)}, u32[]{:S(2)}) collective-permute-start(bf16[1552,128]{1,0:T(8,128)(2,1)} %get-tuple-element.12), channel_id=1, source_target_pairs={{0,16},{8,24},{16,0},{24,8},{1,17},{9,25},{17,1},{25,9},{2,18},{10... | collective-permute-start | bytes 1191944 | tf_op jit(solution)/shard_map/swap/ppermute | solution.py:155
  71.3 4.4 %collective-permute-start.2 = (bf16[1552,128]{1,0:T(8,128)(2,1)}, bf16[1552,128]{1,0:T(8,128)(2,1)S(1)}, u32[]{:S(2)}, u32[]{:S(2)}) collective-permute-start(bf16[1552,128]{1,0:T(8,128)(2,1)} %get-tuple-element.11), channel_id=1, source_target_pairs={{0,24},{8,16},{16,8},{24,0},{1,25},{9,17},{17,9},{25,1},{2,26},{10... | collective-permute-start | bytes 1191944 | tf_op jit(solution)/shard_map/swap/ppermute | solution.py:155
  75.7 11.5 %all-to-all-done.1 = bf16[8,4,1408]{2,1,0:T(4,128)(2,1)S(1)} async-done(((bf16[8,4,1408]{2,1,0:T(4,128)(2,1)}), bf16[8,4,1408]{2,1,0:T(4,128)(2,1)S(1)}, u32[]{:S(2)}, u32[]{:S(2)}) %all-to-all-start.1) | async-done | bytes 90144 | tf_op jit(solution)/shard_map/all_to_all | solution.py:22
  87.9 1.4 multiply_reduce_fusion
  90.0 9.6 %all-to-all-start.2 = ((bf16[8,4,512]{2,1,0:T(4,128)(2,1)}), bf16[8,4,512]{2,1,0:T(4,128)(2,1)S(1)}, u32[]{:S(2)}, u32[]{:S(2)}) async-start(bf16[8,4,512]{2,1,0:T(4,128)(2,1)} %broadcast_in_dim.52), calls=%async_computation.2 | async-start | bytes 65536 | tf_op jit(solution)/shard_map/all_to_all | solution.py:27
  99.6 1.4 collective-permute-done.2
  101.7 1.2 pad_maximum_fusion.1
  102.9 18.0 %all-to-all-done.2 = bf16[8,4,512]{2,1,0:T(4,128)(2,1)S(1)} async-done(((bf16[8,4,512]{2,1,0:T(4,128)(2,1)}), bf16[8,4,512]{2,1,0:T(4,128)(2,1)S(1)}, u32[]{:S(2)}, u32[]{:S(2)}) %all-to-all-start.2) | async-done | bytes 32800 | tf_op jit(solution)/shard_map/all_to_all | solution.py:27
  122.0 16.2 %all_to_all.45 = bf16[8,32,640]{2,1,0:T(8,128)(2,1)S(1)} all-to-all(bf16[8,32,640]{2,1,0:T(8,128)(2,1)S(1)} %broadcast_in_dim.63), channel_id=1, replica_groups=mesh['grp'=2,'far'=8,'near'=4,'tp'=8] {'tp'}, dimensions={0} | all-to-all | bytes 655360 | tf_op jit(solution)/shard_map/all_to_all | solution.py:27
  139.1 4.1 %all-to-all-start.4 = ((bf16[4,32,512]{2,1,0:T(8,128)(2,1)}), bf16[4,32,512]{2,1,0:T(8,128)(2,1)S(1)}, u32[]{:S(2)}, u32[]{:S(2)}) async-start(bf16[4,32,512]{2,1,0:T(8,128)(2,1)} %broadcast_in_dim.64), calls=%async_computation.4 | async-start | bytes 262144 | tf_op jit(solution)/shard_map/all_to_all | solution.py:27
  143.8 4.2 %all-to-all-done.4 = bf16[4,32,512]{2,1,0:T(8,128)(2,1)S(1)} async-done(((bf16[4,32,512]{2,1,0:T(8,128)(2,1)}), bf16[4,32,512]{2,1,0:T(8,128)(2,1)S(1)}, u32[]{:S(2)}, u32[]{:S(2)}) %all-to-all-start.4) | async-done | bytes 131104 | tf_op jit(solution)/shard_map/all_to_all | solution.py:27
  148.6 32.3 %all_to_all.46 = bf16[8,16,640]{2,1,0:T(8,128)(2,1)S(1)} all-to-all(bf16[8,16,640]{2,1,0:T(8,128)(2,1)S(1)} %bitcast.172), channel_id=1, replica_groups=mesh['grp'=2,'far'=8,'near'=4,'tp'=8] {'far'}, dimensions={0} | all-to-all | bytes 327680 | tf_op jit(solution)/shard_map/all_to_all | solution.py:22
  181.7 6.7 %all-to-all-start.6 = ((bf16[8,16,512]{2,1,0:T(8,128)(2,1)}), bf16[8,16,512]{2,1,0:T(8,128)(2,1)S(1)}, u32[]{:S(2)}, u32[]{:S(2)}) async-start(bf16[8,16,512]{2,1,0:T(8,128)(2,1)} %broadcast_in_dim.71), calls=%async_computation.6 | async-start | bytes 262144 | tf_op jit(solution)/shard_map/all_to_all | solution.py:27
  188.5 22.8 %all-to-all-done.6 = bf16[8,16,512]{2,1,0:T(8,128)(2,1)S(1)} async-done(((bf16[8,16,512]{2,1,0:T(8,128)(2,1)}), bf16[8,16,512]{2,1,0:T(8,128)(2,1)S(1)}, u32[]{:S(2)}, u32[]{:S(2)}) %all-to-all-start.6) | async-done | bytes 131104 | tf_op jit(solution)/shard_map/all_to_all | solution.py:27
  212.6 14.4 %all-to-all-start.7 = ((bf16[32,16,128]{2,1,0:T(8,128)(2,1)}), bf16[32,16,128]{2,1,0:T(8,128)(2,1)S(1)}, u32[]{:S(2)}, u32[]{:S(2)}) async-start(bf16[32,16,128]{2,1,0:T(8,128)(2,1)} %bitcast.51), calls=%async_computation.7 | async-start | bytes 262144 | tf_op jit(solution)/shard_map/all_to_all | solution.py:226
  227.1 8.4 %all-to-all-done.7 = bf16[32,16,128]{2,1,0:T(8,128)(2,1)S(1)} async-done(((bf16[32,16,128]{2,1,0:T(8,128)(2,1)}), bf16[32,16,128]{2,1,0:T(8,128)(2,1)S(1)}, u32[]{:S(2)}, u32[]{:S(2)}) %all-to-all-start.7) | async-done | bytes 131104 | tf_op jit(solution)/shard_map/all_to_all | solution.py:226
  235.5 7.4 %all_to_all.47 = bf16[8,16,128]{2,1,0:T(8,128)(2,1)S(1)} all-to-all(bf16[8,16,128]{2,1,0:T(8,128)(2,1)S(1)} %broadcast_in_dim.116), channel_id=1, replica_groups=mesh['grp'=2,'far'=8,'near'=4,'tp'=8] {'tp'}, dimensions={0} | all-to-all | bytes 65536 | tf_op jit(solution)/shard_map/all_to_all | solution.py:27
  (94 shorter events, 12.7 us)
Async XLA Ops:
  0.6 15.1 %copy-start.5 = (bf16[4,3,512]{2,0,1:T(4,128)(2,1)S(1)}, bf16[4,3,512]{2,0,1:T(4,128)(2,1)}, u32[]{:S(2)}) copy-start(bf16[4,3,512]{2,0,1:T(4,128)(2,1)} %param.22) | copy-start | bytes 36868
  0.6 63.7 %copy-start.2 = (bf16[128,2048]{1,0:T(8,128)(2,1)S(1)}, bf16[128,2048]{1,0:T(8,128)(2,1)}, u32[]{:S(2)}) copy-start(bf16[128,2048]{1,0:T(8,128)(2,1)} %param.38) | copy-start | bytes 1572868
  2.9 16.8 %all-to-all-start = ((bf16[4,32,1536]{2,1,0:T(8,128)(2,1)}), bf16[4,32,1536]{2,1,0:T(8,128)(2,1)S(1)}, u32[]{:S(2)}, u32[]{:S(2)}) async-start(bf16[4,32,1536]{2,1,0:T(8,128)(2,1)} %bitcast.171), calls=%async_computation | async-start | bytes 786432 | tf_op jit(solution)/shard_map/all_to_all | solution.py:130
  11.9 53.0 %copy-start.6 = (bf16[512]{0:T(512)(128)(2,1)S(1)}, bf16[512]{0:T(512)(128)(2,1)}, u32[]{:S(2)}) copy-start(bf16[512]{0:T(512)(128)(2,1)} %param.35) | copy-start | bytes 3076
  11.9 53.0 %copy-start.7 = (bf16[128]{0:T(256)(128)(2,1)S(1)}, bf16[128]{0:T(256)(128)(2,1)}, u32[]{:S(2)}) copy-start(bf16[128]{0:T(256)(128)(2,1)} %param.37) | copy-start | bytes 772
  11.9 53.1 %copy-start.4 = (bf16[512,128]{1,0:T(8,128)(2,1)S(1)}, bf16[512,128]{1,0:T(8,128)(2,1)}, u32[]{:S(2)}) copy-start(bf16[512,128]{1,0:T(8,128)(2,1)} %param.36) | copy-start | bytes 393220
  19.7 45.4 %copy-start.1 = (bf16[2048,128]{1,0:T(8,128)(2,1)S(1)}, bf16[2048,128]{1,0:T(8,128)(2,1)}, u32[]{:S(2)}) copy-start(bf16[2048,128]{1,0:T(8,128)(2,1)} %param.39) | copy-start | bytes 1572868
  20.4 66.8 %all-to-all-start.1 = ((bf16[8,4,1408]{2,1,0:T(4,128)(2,1)}), bf16[8,4,1408]{2,1,0:T(4,128)(2,1)S(1)}, u32[]{:S(2)}, u32[]{:S(2)}) async-start(bf16[8,4,1408]{2,1,0:T(4,128)(2,1)} %reshape.201), calls=%async_computation.1 | async-start | bytes 180224 | tf_op jit(solution)/shard_map/all_to_all | solution.py:22
  65.2 22.5 %copy-start.8 = (f32[8]{0:T(128)S(1)}, f32[8]{0:T(128)}, u32[]{:S(2)}) copy-start(f32[8]{0:T(128)} %param.31) | copy-start | bytes 100
  65.2 22.7 %copy-start = (f32[4,8,64,128]{3,2,1,0:T(8,128)S(1)}, f32[4,8,64,128]{3,2,1,0:T(8,128)}, u32[]{:S(2)}) copy-start(f32[4,8,64,128]{3,2,1,0:T(8,128)} %param.24) | copy-start | bytes 3145732
  66.3 33.3 %collective-permute-start = (bf16[1552,128]{1,0:T(8,128)(2,1)}, bf16[1552,128]{1,0:T(8,128)(2,1)S(1)}, u32[]{:S(2)}, u32[]{:S(2)}) collective-permute-start(bf16[1552,128]{1,0:T(8,128)(2,1)} %get-tuple-element.13), channel_id=1, source_target_pairs={{0,8},{8,0},{16,24},{24,16},{1,9},{9,1},{17,25},{25,17},{2,10},{10... | collective-permute-start | bytes 1191944 | tf_op jit(solution)/shard_map/swap/ppermute | solution.py:155
  68.2 31.4 %collective-permute-start.1 = (bf16[1552,128]{1,0:T(8,128)(2,1)}, bf16[1552,128]{1,0:T(8,128)(2,1)S(1)}, u32[]{:S(2)}, u32[]{:S(2)}) collective-permute-start(bf16[1552,128]{1,0:T(8,128)(2,1)} %get-tuple-element.12), channel_id=1, source_target_pairs={{0,16},{8,24},{16,0},{24,8},{1,17},{9,25},{17,1},{25,9},{2,18},{10... | collective-permute-start | bytes 1191944 | tf_op jit(solution)/shard_map/swap/ppermute | solution.py:155
  71.3 29.7 %collective-permute-start.2 = (bf16[1552,128]{1,0:T(8,128)(2,1)}, bf16[1552,128]{1,0:T(8,128)(2,1)S(1)}, u32[]{:S(2)}, u32[]{:S(2)}) collective-permute-start(bf16[1552,128]{1,0:T(8,128)(2,1)} %get-tuple-element.11), channel_id=1, source_target_pairs={{0,24},{8,16},{16,8},{24,0},{1,25},{9,17},{17,9},{25,1},{2,26},{10... | collective-permute-start | bytes 1191944 | tf_op jit(solution)/shard_map/swap/ppermute | solution.py:155
  90.0 30.9 %all-to-all-start.2 = ((bf16[8,4,512]{2,1,0:T(4,128)(2,1)}), bf16[8,4,512]{2,1,0:T(4,128)(2,1)S(1)}, u32[]{:S(2)}, u32[]{:S(2)}) async-start(bf16[8,4,512]{2,1,0:T(4,128)(2,1)} %broadcast_in_dim.52), calls=%async_computation.2 | async-start | bytes 65536 | tf_op jit(solution)/shard_map/all_to_all | solution.py:27
  101.0 0.8 copy-start.3
  139.1 8.9 %all-to-all-start.4 = ((bf16[4,32,512]{2,1,0:T(8,128)(2,1)}), bf16[4,32,512]{2,1,0:T(8,128)(2,1)S(1)}, u32[]{:S(2)}, u32[]{:S(2)}) async-start(bf16[4,32,512]{2,1,0:T(8,128)(2,1)} %broadcast_in_dim.64), calls=%async_computation.4 | async-start | bytes 262144 | tf_op jit(solution)/shard_map/all_to_all | solution.py:27
  181.7 29.5 %all-to-all-start.6 = ((bf16[8,16,512]{2,1,0:T(8,128)(2,1)}), bf16[8,16,512]{2,1,0:T(8,128)(2,1)S(1)}, u32[]{:S(2)}, u32[]{:S(2)}) async-start(bf16[8,16,512]{2,1,0:T(8,128)(2,1)} %broadcast_in_dim.71), calls=%async_computation.6 | async-start | bytes 262144 | tf_op jit(solution)/shard_map/all_to_all | solution.py:27
  212.6 22.8 %all-to-all-start.7 = ((bf16[32,16,128]{2,1,0:T(8,128)(2,1)}), bf16[32,16,128]{2,1,0:T(8,128)(2,1)S(1)}, u32[]{:S(2)}, u32[]{:S(2)}) async-start(bf16[32,16,128]{2,1,0:T(8,128)(2,1)} %bitcast.51), calls=%async_computation.7 | async-start | bytes 262144 | tf_op jit(solution)/shard_map/all_to_all | solution.py:226

commit v3 on v2

--- a/solution.py
+++ b/solution.py
@@ -5,6 +5,7 @@
 from jax import lax
 from jax.experimental import pallas as pl
 from jax.sharding import Mesh, PartitionSpec as P
+
 
 HEAD_DIM = 64
 STATE = 128
@@ -151,8 +152,7 @@
     for step in range(near):
         piece = lax.dynamic_index_in_dim(packed, here ^ step, keepdims=False)
         if step:
-            with jax.named_scope("swap"):
-                piece = lax.ppermute(piece, "near", [(i, i ^ step) for i in range(near)])
+            piece = lax.ppermute(piece, "near", [(i, i ^ step) for i in range(near)])
         pieces.append(piece)
     pieces = jnp.stack(pieces)
     swapped = jnp.stack(
@@ -162,7 +162,12 @@
     own_up = own_up.transpose(0, 2, 1, 3).reshape(near * width, hidden)
     own_down = swapped[:, hidden : 2 * hidden]
     own_out = swapped[:, 2 * hidden : 2 * hidden + w_out.shape[0]]
-    near_gain = swapped[:, 2 * hidden + w_out.shape[0]].reshape(1, near * width)
+    near_gain = swapped[:, 2 * hidden + w_out.shape[0]].reshape(1, near * width).astype(f32)
+    rows = near_tokens.reshape(lax.axis_size("tp"), -1, near * width)
+    own_tokens = rows[lax.axis_index("tp")]
+    own_up, own_down, own_out, near_gain, own_tokens = lax.optimization_barrier(
+        (own_up, own_down, own_out, near_gain, own_tokens)
+    )
 
     cuts, at = [], 0
     for size in (w_gate.shape[1], w_value.shape[1], w_key.shape[1], w_query.shape[1], head_count):
@@ -197,35 +202,36 @@
     gated_rows = mixer_y * jax.nn.silu(gate_raw * inverse)
     gated_low = (gated_rows * inner_gain.astype(f32)).astype(bf16)
 
-    all_low = from_everyone(gated_low, "far").reshape(far * seqs, -1)
+    all_low = from_everyone(gated_low, "far")
+    all_low = all_low.reshape(far * seqs, -1)
     ungained = all_low.astype(f32) / inner_gain.astype(f32)
     gated_squares = hi_lo(jnp.sum(ungained * ungained, axis=1, keepdims=True))
     out_part = [product(all_low, own_out[i], bf16) for i in range(near)]
-    shared = from_everyone(jnp.concatenate([*out_part, gated_squares], axis=1), "tp")
-    shared = shared.astype(f32).sum(axis=0)
+    tp = lax.axis_size("tp")
+    shared = scattered_sum(jnp.concatenate([*out_part, gated_squares], axis=1), "tp")
     gated_total = jnp.sum(shared[:, near * width :], axis=1, keepdims=True)
     residual = (
-        near_tokens.astype(f32)
+        own_tokens.astype(f32)
         + shared[:, : near * width] * lax.rsqrt(gated_total / inner + epsilon)
     ).astype(bf16)
 
-    residual = from_everyone(residual, "near").reshape(batch, near * width)
+    residual = from_everyone(residual, ("near", "tp")).reshape(batch, near * width)
     residual_wide = residual.astype(f32)
-    hidden_low = (residual_wide * near_gain.astype(f32)).astype(bf16)
+    hidden_low = (residual_wide * near_gain).astype(bf16)
     row_squares = jnp.sum(residual_wide * residual_wide, axis=1, keepdims=True)
     up_part = jnp.concatenate([product(hidden_low, own_up, bf16), hi_lo(row_squares)], axis=1)
+    own_rows = residual.reshape(tp, batch // tp, near, width).swapaxes(1, 2)
+    own_rows = own_rows[lax.axis_index("tp"), lax.axis_index("near")]
+    up_part, own_rows = lax.optimization_barrier((up_part, own_rows))
     up_mine = scattered_sum(up_part, "far")
     up_share, square_share = up_mine[:, :hidden], jnp.sum(up_mine[:, hidden:], axis=1, keepdims=True)
     active = jnp.square(
         jax.nn.relu(up_share * lax.rsqrt(square_share / model + epsilon))
     ).astype(bf16)
     active = from_everyone(active, "far").reshape(batch, hidden)
-    tp = lax.axis_size("tp")
     down_part = jnp.stack([product(active, own_down[i], bf16) for i in range(near)])
     down_part = down_part.reshape(near * tp, batch // tp, width)
     down_sum = lax.all_to_all(down_part, ("near", "tp"), 0, 0, tiled=True).astype(f32).sum(axis=0)
-    own_rows = residual.reshape(tp, batch // tp, near, width).swapaxes(1, 2)
-    own_rows = own_rows[lax.axis_index("tp"), lax.axis_index("near")]
     finished = (own_rows.astype(f32) + down_sum).astype(bf16)
     finished = from_everyone(finished, "tp").reshape(near, far, seqs, width)
     return (finished.swapaxes(0, 1).reshape(batch, width), next_state)

time: 245 us -> 264 us (1.078)
  blocking collectives: 55.9 us -> 124 us
  waiting for transfers between devices: 70.1 us -> 46.4 us
  starting transfers between devices: 97.2 us -> 77.3 us
    all_to_all x2 -> x3, blocking collectives: 23.6 us -> 59.8 us  [from_everyone(): return lax.all_to_all(copies, along, 0, 0, tiled=True)]
    all_to_all x3 -> x1, waiting for transfers between devices: 45 us -> 19.8 us  [from_everyone(): return lax.all_to_all(copies, along, 0, 0, tiled=True)]
    all_to_all x0 -> x1, blocking collectives: none -> 17.7 us  [per_device(): lax.all_to_all(down_part, ('near', 'tp'), 0, 0, tiled=True).astype(f32)]
    all_to_all x1 -> x0, starting transfers between devices: 14.4 us -> none  [per_device(): lax.all_to_all(down_part, ('near', 'tp'), 0, 0, tiled=True).astype(f32)]
    all_to_all x1 -> x2, blocking collectives: 32.3 us -> 46.2 us  [scattered_sum(): lax.all_to_all(parts, along, 0, 0, tiled=True).astype(f32).sum(axis=0)]
    all_to_all x1, waiting for transfers between devices: 11.5 us -> 21.1 us  [scattered_sum(): lax.all_to_all(parts, along, 0, 0, tiled=True).astype(f32).sum(axis=0)]
    all_to_all x1 -> x0, waiting for transfers between devices: 8.38 us -> none  [per_device(): lax.all_to_all(down_part, ('near', 'tp'), 0, 0, tiled=True).astype(f32)]
    all_to_all x3 -> x1, starting transfers between devices: 20.4 us -> 14.8 us  [from_everyone(): return lax.all_to_all(copies, along, 0, 0, tiled=True)]
  transfers between devices with their start and end apart: 9 -> 6, of which waited for: 7 -> 3; matrix products, arithmetic and copies ran while one was open for 4% -> 2% of each run, Pallas kernels for 0% -> 0%
where the time goes in v3:
time: 264 us
  blocking collectives  124 us (47%)
  starting transfers between devices  77.3 us (29%)
  waiting for transfers between devices  46.4 us (18%)
  other arithmetic  6.31 us (2%)
  local copies, waits for them, and re-layouts  5.15 us (2%)
    all_to_all x3, blocking collectives, from_everyone(): return lax.all_to_all(copies, along, 0, 0, tiled=True)  59.8 us
    all_to_all x2, blocking collectives, scattered_sum(): lax.all_to_all(parts, along, 0, 0, tiled=True).astype(f32).sum(axis=0)  46.2 us
    all_to_all x1, starting transfers between devices, scattered_sum(): lax.all_to_all(parts, along, 0, 0, tiled=True).astype(f32).sum(axis=0)  44 us
    all_to_all x1, waiting for transfers between devices, scattered_sum(): lax.all_to_all(parts, along, 0, 0, tiled=True).astype(f32).sum(axis=0)  21.1 us
    all_to_all x1, waiting for transfers between devices, from_everyone(): return lax.all_to_all(copies, along, 0, 0, tiled=True)  19.8 us
    all_to_all x1, blocking collectives, per_device(): lax.all_to_all(down_part, ('near', 'tp'), 0, 0, tiled=True).astype(f32)  17.7 us
    all_to_all x1, starting transfers between devices, from_everyone(): return lax.all_to_all(copies, along, 0, 0, tiled=True)  14.8 us
    ppermute x3, starting transfers between devices, per_device(): piece = lax.ppermute(piece, 'near', [(i, i ^ step) for i in range(near)])  9.36 us
  transfers between devices with their start and end apart: 6, of which 3 were waited for; matrix products, arithmetic and copies ran while one was open for 2% of the time, Pallas kernels for 0%

profile of v3, /device:TPU:33, one launch (start us, length us, event | category | flops | bytes accessed | tf_op | source)
XLA Modules:
  0.0 263.8 jit_solution(5287465521854171424)
XLA Ops:
  0.6 2.2 project.1
  2.9 9.2 %all-to-all-start = ((bf16[4,32,1536]{2,1,0:T(8,128)(2,1)}), bf16[4,32,1536]{2,1,0:T(8,128)(2,1)S(1)}, u32[]{:S(2)}, u32[]{:S(2)}) async-start(bf16[4,32,1536]{2,1,0:T(8,128)(2,1)} %bitcast.175), calls=%async_computation | async-start | bytes 786432 | tf_op jit(solution)/shard_map/all_to_all | solution.py:131
  12.1 0.7 convert_element_type.160
  12.8 0.7 broadcast_subtract_fusion
  14.3 5.5 %all-to-all-done = bf16[4,32,1536]{2,1,0:T(8,128)(2,1)S(1)} async-done(((bf16[4,32,1536]{2,1,0:T(8,128)(2,1)}), bf16[4,32,1536]{2,1,0:T(8,128)(2,1)S(1)}, u32[]{:S(2)}, u32[]{:S(2)}) %all-to-all-start) | async-done | bytes 393248 | tf_op jit(solution)/shard_map/all_to_all | solution.py:131
  20.3 3.4 %collective-permute-start.2 = (bf16[1552,128]{1,0:T(8,128)(2,1)S(1)}, bf16[1552,128]{1,0:T(8,128)(2,1)S(1)}, u32[]{:S(2)}, u32[]{:S(2)}) collective-permute-start(bf16[1552,128]{1,0:T(8,128)(2,1)S(1)} %get-tuple-element.28), channel_id=1, source_target_pairs={{0,24},{8,16},{16,8},{24,0},{1,25},{9,17},{17,9},{25,1},{2,26},{10... | collective-permute-start | bytes 1191944 | tf_op jit(solution)/shard_map/ppermute | solution.py:155
  23.7 2.0 collective-permute-start.1
  25.6 4.0 %collective-permute-start = (bf16[1552,128]{1,0:T(8,128)(2,1)S(1)}, bf16[1552,128]{1,0:T(8,128)(2,1)S(1)}, u32[]{:S(2)}, u32[]{:S(2)}) collective-permute-start(bf16[1552,128]{1,0:T(8,128)(2,1)S(1)} %get-tuple-element.30), channel_id=1, source_target_pairs={{0,8},{8,0},{16,24},{24,16},{1,9},{9,1},{17,25},{25,17},{2,10},{10... | collective-permute-start | bytes 1191944 | tf_op jit(solution)/shard_map/ppermute | solution.py:155
  29.7 0.7 reshape.205
  30.4 44.0 %all-to-all-start.1 = ((bf16[8,4,1408]{2,1,0:T(4,128)(2,1)}), bf16[8,4,1408]{2,1,0:T(4,128)(2,1)S(1)}, u32[]{:S(2)}, u32[]{:S(2)}) async-start(bf16[8,4,1408]{2,1,0:T(4,128)(2,1)} %reshape.205), calls=%async_computation.1 | async-start | bytes 180224 | tf_op jit(solution)/shard_map/all_to_all | solution.py:23
  75.0 21.1 %all-to-all-done.1 = bf16[8,4,1408]{2,1,0:T(4,128)(2,1)S(1)} async-done(((bf16[8,4,1408]{2,1,0:T(4,128)(2,1)}), bf16[8,4,1408]{2,1,0:T(4,128)(2,1)S(1)}, u32[]{:S(2)}, u32[]{:S(2)}) %all-to-all-start.1) | async-done | bytes 90144 | tf_op jit(solution)/shard_map/all_to_all | solution.py:23
  96.8 2.6 multiply_reduce_fusion
  99.5 0.6 broadcast_in_dim.53
  100.2 14.8 %all-to-all-start.2 = ((bf16[8,4,512]{2,1,0:T(4,128)(2,1)}), bf16[8,4,512]{2,1,0:T(4,128)(2,1)S(1)}, u32[]{:S(2)}, u32[]{:S(2)}) async-start(bf16[8,4,512]{2,1,0:T(4,128)(2,1)} %broadcast_in_dim.53), calls=%async_computation.2 | async-start | bytes 65536 | tf_op jit(solution)/shard_map/all_to_all | solution.py:28
  115.0 1.1 fusion.40
  116.1 0.4 copy.79
  116.6 19.8 %all-to-all-done.2 = bf16[8,4,512]{2,1,0:T(4,128)(2,1)S(1)} async-done(((bf16[8,4,512]{2,1,0:T(4,128)(2,1)}), bf16[8,4,512]{2,1,0:T(4,128)(2,1)S(1)}, u32[]{:S(2)}, u32[]{:S(2)}) %all-to-all-start.2) | async-done | bytes 32800 | tf_op jit(solution)/shard_map/all_to_all | solution.py:28
  137.4 14.6 %all_to_all.45 = bf16[8,4,640]{2,1,0:T(4,128)(2,1)S(1)} all-to-all(bf16[8,4,640]{2,1,0:T(4,128)(2,1)S(1)} %reshape.209), channel_id=1, replica_groups=mesh['grp'=2,'far'=8,'near'=4,'tp'=8] {'tp'}, dimensions={0} | all-to-all | bytes 81920 | tf_op jit(solution)/shard_map/all_to_all | solution.py:23
  152.3 20.6 %all_to_all.46 = bf16[32,4,512]{2,1,0:T(4,128)(2,1)S(1)} all-to-all(bf16[32,4,512]{2,1,0:T(4,128)(2,1)S(1)} %broadcast_in_dim.57), channel_id=1, replica_groups=mesh['grp'=2,'far'=8,'near'=4,'tp'=8] {'near','tp'}, dimensions={0} | all-to-all | bytes 262144 | tf_op jit(solution)/shard_map/all_to_all | solution.py:28
  173.6 31.6 %all_to_all.47 = bf16[8,16,640]{2,1,0:T(8,128)(2,1)S(1)} all-to-all(bf16[8,16,640]{2,1,0:T(8,128)(2,1)S(1)} %bitcast.176), channel_id=1, replica_groups=mesh['grp'=2,'far'=8,'near'=4,'tp'=8] {'far'}, dimensions={0} | all-to-all | bytes 327680 | tf_op jit(solution)/shard_map/all_to_all | solution.py:23
  205.4 31.7 %all_to_all.48 = bf16[8,16,512]{2,1,0:T(8,128)(2,1)S(1)} all-to-all(bf16[8,16,512]{2,1,0:T(8,128)(2,1)S(1)} %broadcast_in_dim.68), channel_id=1, replica_groups=mesh['grp'=2,'far'=8,'near'=4,'tp'=8] {'far'}, dimensions={0} | all-to-all | bytes 262144 | tf_op jit(solution)/shard_map/all_to_all | solution.py:28
  237.9 17.7 %all_to_all.49 = bf16[32,16,128]{2,1,0:T(8,128)(2,1)S(1)} all-to-all(bf16[32,16,128]{2,1,0:T(8,128)(2,1)S(1)} %bitcast.178), channel_id=1, replica_groups=mesh['grp'=2,'far'=8,'near'=4,'tp'=8] {'near','tp'}, dimensions={0} | all-to-all | bytes 262144 | tf_op jit(solution)/shard_map/all_to_all | solution.py:234
  255.7 7.4 %all_to_all.50 = bf16[8,16,128]{2,1,0:T(8,128)(2,1)S(1)} all-to-all(bf16[8,16,128]{2,1,0:T(8,128)(2,1)S(1)} %broadcast_in_dim.69), channel_id=1, replica_groups=mesh['grp'=2,'far'=8,'near'=4,'tp'=8] {'tp'}, dimensions={0} | all-to-all | bytes 65536 | tf_op jit(solution)/shard_map/all_to_all | solution.py:28
  263.1 0.6 copy.87
  (105 shorter events, 5.6 us)
Async XLA Ops:
  0.6 12.9 %copy-start.3 = (bf16[128,2048]{1,0:T(8,128)(2,1)S(1)}, bf16[128,2048]{1,0:T(8,128)(2,1)}, u32[]{:S(2)}) copy-start(bf16[128,2048]{1,0:T(8,128)(2,1)} %param.38) | copy-start | bytes 1572868
  2.9 11.2 %copy-start.11 = (f32[8]{0:T(128)S(1)}, f32[8]{0:T(128)}, u32[]{:S(2)}) copy-start(f32[8]{0:T(128)} %param.32) | copy-start | bytes 100
  2.9 11.2 %copy-start.8 = (bf16[4,2,128]{2,1,0:T(2,128)(2,1)S(1)}, bf16[4,2,128]{2,1,0:T(2,128)(2,1)}, u32[]{:S(2)}) copy-start(bf16[4,2,128]{2,1,0:T(2,128)(2,1)} %param.34) | copy-start | bytes 6148
  2.9 11.2 %copy-start.5 = (bf16[4,512]{1,0:T(4,128)(2,1)S(1)}, bf16[4,512]{1,0:T(4,128)(2,1)}, u32[]{:S(2)}) copy-start(bf16[4,512]{1,0:T(4,128)(2,1)} %param.33) | copy-start | bytes 12292
  2.9 11.3 %copy-start.7 = (bf16[4,3,2,128]{3,2,1,0:T(2,128)(2,1)S(1)}, bf16[4,3,2,128]{3,2,1,0:T(2,128)(2,1)}, u32[]{:S(2)}) copy-start(bf16[4,3,2,128]{3,2,1,0:T(2,128)(2,1)} %param.23) | copy-start | bytes 18436
  2.9 11.3 %copy-start.6 = (bf16[4,3,512]{2,0,1:T(4,128)(2,1)S(1)}, bf16[4,3,512]{2,0,1:T(4,128)(2,1)}, u32[]{:S(2)}) copy-start(bf16[4,3,512]{2,0,1:T(4,128)(2,1)} %param.22) | copy-start | bytes 36868
  2.9 17.0 %copy-start.9 = (bf16[128]{0:T(256)(128)(2,1)S(1)}, bf16[128]{0:T(256)(128)(2,1)}, u32[]{:S(2)}) copy-start(bf16[128]{0:T(256)(128)(2,1)} %param.37) | copy-start | bytes 772
  2.9 17.0 %copy-start.4 = (bf16[512,128]{1,0:T(8,128)(2,1)S(1)}, bf16[512,128]{1,0:T(8,128)(2,1)}, u32[]{:S(2)}) copy-start(bf16[512,128]{1,0:T(8,128)(2,1)} %param.36) | copy-start | bytes 393220
  2.9 16.9 %all-to-all-start = ((bf16[4,32,1536]{2,1,0:T(8,128)(2,1)}), bf16[4,32,1536]{2,1,0:T(8,128)(2,1)S(1)}, u32[]{:S(2)}, u32[]{:S(2)}) async-start(bf16[4,32,1536]{2,1,0:T(8,128)(2,1)} %bitcast.175), calls=%async_computation | async-start | bytes 786432 | tf_op jit(solution)/shard_map/all_to_all | solution.py:131
  13.5 6.5 %copy-start.2 = (bf16[2048,128]{1,0:T(8,128)(2,1)S(1)}, bf16[2048,128]{1,0:T(8,128)(2,1)}, u32[]{:S(2)}) copy-start(bf16[2048,128]{1,0:T(8,128)(2,1)} %param.39) | copy-start | bytes 1572868
  20.3 54.1 %collective-permute-start.2 = (bf16[1552,128]{1,0:T(8,128)(2,1)S(1)}, bf16[1552,128]{1,0:T(8,128)(2,1)S(1)}, u32[]{:S(2)}, u32[]{:S(2)}) collective-permute-start(bf16[1552,128]{1,0:T(8,128)(2,1)S(1)} %get-tuple-element.28), channel_id=1, source_target_pairs={{0,24},{8,16},{16,8},{24,0},{1,25},{9,17},{17,9},{25,1},{2,26},{10... | collective-permute-start | bytes 1191944 | tf_op jit(solution)/shard_map/ppermute | solution.py:155
  23.7 50.7 %collective-permute-start.1 = (bf16[1552,128]{1,0:T(8,128)(2,1)S(1)}, bf16[1552,128]{1,0:T(8,128)(2,1)S(1)}, u32[]{:S(2)}, u32[]{:S(2)}) collective-permute-start(bf16[1552,128]{1,0:T(8,128)(2,1)S(1)} %get-tuple-element.29), channel_id=1, source_target_pairs={{0,16},{8,24},{16,0},{24,8},{1,17},{9,25},{17,1},{25,9},{2,18},{10... | collective-permute-start | bytes 1191944 | tf_op jit(solution)/shard_map/ppermute | solution.py:155
  25.6 48.8 %collective-permute-start = (bf16[1552,128]{1,0:T(8,128)(2,1)S(1)}, bf16[1552,128]{1,0:T(8,128)(2,1)S(1)}, u32[]{:S(2)}, u32[]{:S(2)}) collective-permute-start(bf16[1552,128]{1,0:T(8,128)(2,1)S(1)} %get-tuple-element.30), channel_id=1, source_target_pairs={{0,8},{8,0},{16,24},{24,16},{1,9},{9,1},{17,25},{25,17},{2,10},{10... | collective-permute-start | bytes 1191944 | tf_op jit(solution)/shard_map/ppermute | solution.py:155
  30.4 65.7 %all-to-all-start.1 = ((bf16[8,4,1408]{2,1,0:T(4,128)(2,1)}), bf16[8,4,1408]{2,1,0:T(4,128)(2,1)S(1)}, u32[]{:S(2)}, u32[]{:S(2)}) async-start(bf16[8,4,1408]{2,1,0:T(4,128)(2,1)} %reshape.205), calls=%async_computation.1 | async-start | bytes 180224 | tf_op jit(solution)/shard_map/all_to_all | solution.py:23
  74.7 21.9 %copy-start.10 = (f32[8]{0:T(128)S(1)}, f32[8]{0:T(128)}, u32[]{:S(2)}) copy-start(f32[8]{0:T(128)} %param.31) | copy-start | bytes 100
  100.2 36.2 %all-to-all-start.2 = ((bf16[8,4,512]{2,1,0:T(4,128)(2,1)}), bf16[8,4,512]{2,1,0:T(4,128)(2,1)S(1)}, u32[]{:S(2)}, u32[]{:S(2)}) async-start(bf16[8,4,512]{2,1,0:T(4,128)(2,1)} %broadcast_in_dim.53), calls=%async_computation.2 | async-start | bytes 65536 | tf_op jit(solution)/shard_map/all_to_all | solution.py:28
  116.5 20.2 %copy-start.1 = (bf16[4,512,128]{2,1,0:T(8,128)(2,1)S(1)}, bf16[4,512,128]{2,1,0:T(8,128)(2,1)}, u32[]{:S(2)}) copy-start(bf16[4,512,128]{2,1,0:T(8,128)(2,1)} %get-tuple-element.10) | copy-start | bytes 1572868
  172.8 64.4 %copy-start = (bf16[4,512,128]{2,1,0:T(8,128)(2,1)S(1)}, bf16[4,512,128]{2,1,0:T(8,128)(2,1)}, u32[]{:S(2)}) copy-start(bf16[4,512,128]{2,1,0:T(8,128)(2,1)} %get-tuple-element.15) | copy-start | bytes 1572868

commit v4 on v2

--- a/solution.py
+++ b/solution.py
@@ -6,6 +6,7 @@
 from jax.experimental import pallas as pl
 from jax.sharding import Mesh, PartitionSpec as P
 
+
 HEAD_DIM = 64
 STATE = 128
 CONV_WIDTH = 4
@@ -35,7 +36,7 @@
 
 
 def project_kernel(
-    far, near, seqs, tokens_ref, gain_ref, gate_ref, value_ref, key_ref, query_ref, step_ref, sent_ref
+    far, near, seqs, tokens_ref, gain_ref, gate_ref, value_ref, key_ref, query_ref, step_ref, sent_ref, rows_ref
 ):
     batch, width = tokens_ref.shape
     to = lax.broadcasted_iota(jnp.int32, (batch, batch), 0)
@@ -63,16 +64,19 @@
     high = squares.astype(bf16).astype(f32)
     lane = lax.broadcasted_iota(jnp.int32, (batch, LANES), 1)
     steps = jnp.where(lane == heads, high, jnp.where(lane == heads + 1, squares - high, steps))
-    sent_ref[:, column : column + LANES] = steps.astype(bf16)
-    sent_ref[:, column + LANES :] = wide.astype(bf16)
+    sent_ref[:, column:] = steps.astype(bf16)
+    rows_ref[...] = wide.astype(bf16)
 
 
 def project(tokens, norm_gain, w_gate, w_value, w_key, w_query, w_step, far, near):
     batch, width = tokens.shape
-    columns = sum(w.shape[1] for w in (w_gate, w_value, w_key, w_query)) + LANES + width
+    columns = sum(w.shape[1] for w in (w_gate, w_value, w_key, w_query)) + LANES
     return pl.pallas_call(
         functools.partial(project_kernel, far, near, batch // (far * near)),
-        out_shape=jax.ShapeDtypeStruct((batch, columns), bf16),
+        out_shape=(
+            jax.ShapeDtypeStruct((batch, columns), bf16),
+            jax.ShapeDtypeStruct((batch, width), bf16),
+        ),
         cost_estimate=pl.CostEstimate(
             flops=2 * batch * width * columns,
             bytes_accessed=2 * columns * (batch + width),
@@ -125,11 +129,10 @@
     inner = w_gate.shape[1] * lax.axis_size("tp")
     seqs = batch // (far * near)
 
-    sent = project(tokens, norm_gain, w_gate, w_value, w_key, w_query, w_step, far, near)
-    cols = sent.shape[1] - width
-    came = lax.all_to_all(sent.reshape(near, -1, cols + width), "near", 0, 0, tiled=True)
-    near_sum = came[:, :, :cols].astype(f32).sum(axis=0).astype(bf16)
-    near_tokens = came[:, :, cols:].swapaxes(0, 1).reshape(-1, near * width)
+    sent, token_rows = project(
+        tokens, norm_gain, w_gate, w_value, w_key, w_query, w_step, far, near
+    )
+    near_sum = scattered_sum(sent, "near").astype(bf16)
     mine = scattered_sum(near_sum, "far")
 
     hidden = w_up.shape[1] // near
@@ -142,6 +145,7 @@
             w_up.reshape(width, near, blocks, width).transpose(1, 2, 0, 3).reshape(near, -1, width),
             w_down.reshape(near, -1, width),
             jnp.broadcast_to(w_out[None], (near, *w_out.shape)),
+            token_rows.reshape(near, -1, width),
             jnp.broadcast_to(extra[None], (near, *extra.shape)),
         ],
         axis=1,
@@ -151,8 +155,7 @@
     for step in range(near):
         piece = lax.dynamic_index_in_dim(packed, here ^ step, keepdims=False)
         if step:
-            with jax.named_scope("swap"):
-                piece = lax.ppermute(piece, "near", [(i, i ^ step) for i in range(near)])
+            piece = lax.ppermute(piece, "near", [(i, i ^ step) for i in range(near)])
         pieces.append(piece)
     pieces = jnp.stack(pieces)
     swapped = jnp.stack(
@@ -162,7 +165,9 @@
     own_up = own_up.transpose(0, 2, 1, 3).reshape(near * width, hidden)
     own_down = swapped[:, hidden : 2 * hidden]
     own_out = swapped[:, 2 * hidden : 2 * hidden + w_out.shape[0]]
-    near_gain = swapped[:, 2 * hidden + w_out.shape[0]].reshape(1, near * width)
+    at = 2 * hidden + w_out.shape[0]
+    near_tokens = swapped[:, at : at + batch // near].swapaxes(0, 1).reshape(-1, near * width)
+    near_gain = swapped[:, at + batch // near].reshape(1, near * width).astype(f32)
 
     cuts, at = [], 0
     for size in (w_gate.shape[1], w_value.shape[1], w_key.shape[1], w_query.shape[1], head_count):
@@ -186,18 +191,24 @@
     key_heads = jnp.repeat(key_query[:, 0].reshape(seqs, group_count, STATE), per_group, axis=1)
     query_heads = jnp.repeat(key_query[:, 1].reshape(seqs, group_count, STATE), per_group, axis=1)
     step_size = jax.nn.softplus(step_raw * inverse + step_bias)
-    rate_now = -jnp.exp(decay_log) * step_size
-    next_state = (
-        ssm_state * jnp.exp(rate_now)[:, :, None, None]
-        + (step_size[:, :, None] * mixed_values)[:, :, :, None] * key_heads[:, :, None, :]
-    )
-    mixer_y = jnp.sum(next_state * query_heads[:, :, None, :], axis=3).reshape(
-        seqs, head_count * HEAD_DIM
-    )
+    decay = jnp.exp(-jnp.exp(decay_log) * step_size)
+    fed = step_size[:, :, None] * mixed_values
+    overlap = jnp.sum(key_heads * query_heads, axis=2)
+    mixer_y = (
+        decay[:, :, None] * jnp.sum(ssm_state * query_heads[:, :, None, :], axis=3)
+        + fed * overlap[:, :, None]
+    ).reshape(seqs, head_count * HEAD_DIM)
     gated_rows = mixer_y * jax.nn.silu(gate_raw * inverse)
     gated_low = (gated_rows * inner_gain.astype(f32)).astype(bf16)
-
-    all_low = from_everyone(gated_low, "far").reshape(far * seqs, -1)
+    gated_low, old_state = lax.optimization_barrier((gated_low, ssm_state))
+    next_state = old_state * decay[:, :, None, None] + fed[:, :, :, None] * key_heads[:, :, None, :]
+    picks = [here == i for i in range(near)]
+    own_up, own_down, own_out, near_gain, near_tokens, next_state, picks = lax.optimization_barrier(
+        (own_up, own_down, own_out, near_gain, near_tokens, next_state, picks)
+    )
+
+    all_low = from_everyone(gated_low, "far")
+    all_low = all_low.reshape(far * seqs, -1)
     ungained = all_low.astype(f32) / inner_gain.astype(f32)
     gated_squares = hi_lo(jnp.sum(ungained * ungained, axis=1, keepdims=True))
     out_part = [product(all_low, own_out[i], bf16) for i in range(near)]
@@ -211,23 +222,23 @@
 
     residual = from_everyone(residual, "near").reshape(batch, near * width)
     residual_wide = residual.astype(f32)
-    hidden_low = (residual_wide * near_gain.astype(f32)).astype(bf16)
+    hidden_low = (residual_wide * near_gain).astype(bf16)
     row_squares = jnp.sum(residual_wide * residual_wide, axis=1, keepdims=True)
     up_part = jnp.concatenate([product(hidden_low, own_up, bf16), hi_lo(row_squares)], axis=1)
+    own_rows = residual[:, :width]
+    for i in range(1, near):
+        own_rows = jnp.where(picks[i], residual[:, i * width : (i + 1) * width], own_rows)
+    up_part, own_rows = lax.optimization_barrier((up_part, own_rows))
     up_mine = scattered_sum(up_part, "far")
     up_share, square_share = up_mine[:, :hidden], jnp.sum(up_mine[:, hidden:], axis=1, keepdims=True)
     active = jnp.square(
         jax.nn.relu(up_share * lax.rsqrt(square_share / model + epsilon))
     ).astype(bf16)
     active = from_everyone(active, "far").reshape(batch, hidden)
-    tp = lax.axis_size("tp")
     down_part = jnp.stack([product(active, own_down[i], bf16) for i in range(near)])
-    down_part = down_part.reshape(near * tp, batch // tp, width)
-    down_sum = lax.all_to_all(down_part, ("near", "tp"), 0, 0, tiled=True).astype(f32).sum(axis=0)
-    own_rows = residual.reshape(tp, batch // tp, near, width).swapaxes(1, 2)
-    own_rows = own_rows[lax.axis_index("tp"), lax.axis_index("near")]
-    finished = (own_rows.astype(f32) + down_sum).astype(bf16)
-    finished = from_everyone(finished, "tp").reshape(near, far, seqs, width)
+    down_sum = lax.all_to_all(down_part, "near", 0, 0, tiled=True).astype(f32).sum(axis=0)
+    down_sum = from_everyone(down_sum.astype(bf16), "tp").astype(f32).sum(axis=0)
+    finished = (own_rows.astype(f32) + down_sum).astype(bf16).reshape(near, far, seqs, width)
     return (finished.swapaxes(0, 1).reshape(batch, width), next_state)
 
 

time: 245 us -> 259 us (1.057)
  blocking collectives: 55.9 us -> 124 us
  waiting for transfers between devices: 70.1 us -> 44.8 us
  starting transfers between devices: 97.2 us -> 75 us
  other arithmetic: 8.83 us -> 4.16 us
    all_to_all x2 -> x4, blocking collectives: 23.6 us -> 82.1 us  [from_everyone(): return lax.all_to_all(copies, along, 0, 0, tiled=True)]
    all_to_all x3 -> x1, waiting for transfers between devices: 45 us -> 20.1 us  [from_everyone(): return lax.all_to_all(copies, along, 0, 0, tiled=True)]
    all_to_all x2 -> x0, starting transfers between devices: 23.4 us -> none  [the longest x1 14.4 us: per_device(): lax.all_to_all(down_part, ('near', 'tp'), 0, 0, tiled=True).astype(f32)]
    all_to_all x1 -> x2, waiting for transfers between devices: 11.5 us -> 24.7 us  [scattered_sum(): lax.all_to_all(parts, along, 0, 0, tiled=True).astype(f32).sum(axis=0)]
    all_to_all x2 -> x0, waiting for transfers between devices: 12.2 us -> none  [the longest x1 8.38 us: per_device(): lax.all_to_all(down_part, ('near', 'tp'), 0, 0, tiled=True).astype(f32)]
    all_to_all x0 -> x1, blocking collectives: none -> 10.4 us  [per_device(): lax.all_to_all(down_part, 'near', 0, 0, tiled=True).astype(f32).sum(axis=0)]
    all_to_all x1 -> x2, starting transfers between devices: 44 us -> 52.6 us  [scattered_sum(): lax.all_to_all(parts, along, 0, 0, tiled=True).astype(f32).sum(axis=0)]
    all_to_all x3 -> x1, starting transfers between devices: 20.4 us -> 13.3 us  [from_everyone(): return lax.all_to_all(copies, along, 0, 0, tiled=True)]
  transfers between devices with their start and end apart: 9 -> 6, of which waited for: 7 -> 3; matrix products, arithmetic and copies ran while one was open for 4% -> 2% of each run, Pallas kernels for 0% -> 0%
where the time goes in v4:
time: 259 us; the launch traced here: 258 us
  blocking collectives  124 us (48%)
  starting transfers between devices  75 us (29%)
  waiting for transfers between devices  44.8 us (17%)
  local copies, waits for them, and re-layouts  5.89 us (2%)
  other arithmetic  4.16 us (2%)
    all_to_all x4, blocking collectives, from_everyone(): return lax.all_to_all(copies, along, 0, 0, tiled=True)  82.1 us
    all_to_all x2, starting transfers between devices, scattered_sum(): lax.all_to_all(parts, along, 0, 0, tiled=True).astype(f32).sum(axis=0)  52.6 us
    all_to_all x1, blocking collectives, scattered_sum(): lax.all_to_all(parts, along, 0, 0, tiled=True).astype(f32).sum(axis=0)  31.2 us
    all_to_all x2, waiting for transfers between devices, scattered_sum(): lax.all_to_all(parts, along, 0, 0, tiled=True).astype(f32).sum(axis=0)  24.7 us
    all_to_all x1, waiting for transfers between devices, from_everyone(): return lax.all_to_all(copies, along, 0, 0, tiled=True)  20.1 us
    all_to_all x1, starting transfers between devices, from_everyone(): return lax.all_to_all(copies, along, 0, 0, tiled=True)  13.3 us
    all_to_all x1, blocking collectives, per_device(): lax.all_to_all(down_part, 'near', 0, 0, tiled=True).astype(f32).sum(axis=0)  10.4 us
    ppermute x3, starting transfers between devices, per_device(): piece = lax.ppermute(piece, 'near', [(i, i ^ step) for i in range(near)])  9.15 us
  transfers between devices with their start and end apart: 6, of which 3 were waited for; matrix products, arithmetic and copies ran while one was open for 2% of the time, Pallas kernels for 0%

profile of v4, /device:TPU:33, one launch (start us, length us, event | category | flops | bytes accessed | tf_op | source)
XLA Modules:
  0.0 258.5 jit_solution(10314661198900756312)
XLA Ops:
  0.7 2.2 project.1
  2.8 9.0 %all-to-all-start = ((bf16[4,32,1408]{2,1,0:T(8,128)(2,1)}), bf16[4,32,1408]{2,1,0:T(8,128)(2,1)S(1)}, u32[]{:S(2)}, u32[]{:S(2)}) async-start(bf16[4,32,1408]{2,1,0:T(8,128)(2,1)} %bitcast.186), calls=%async_computation | async-start | bytes 720896 | tf_op jit(solution)/shard_map/all_to_all | solution.py:23
  11.8 1.5 reshape.203
  13.8 0.4 copy-done.2
  14.5 3.8 %all-to-all-done = bf16[4,32,1408]{2,1,0:T(8,128)(2,1)S(1)} async-done(((bf16[4,32,1408]{2,1,0:T(8,128)(2,1)}), bf16[4,32,1408]{2,1,0:T(8,128)(2,1)S(1)}, u32[]{:S(2)}, u32[]{:S(2)}) %all-to-all-start) | async-done | bytes 360480 | tf_op jit(solution)/shard_map/all_to_all | solution.py:23
  18.5 2.4 collective-permute-start.1
  21.0 4.8 %collective-permute-start.2 = (bf16[1584,128]{1,0:T(8,128)(2,1)S(1)}, bf16[1584,128]{1,0:T(8,128)(2,1)S(1)}, u32[]{:S(2)}, u32[]{:S(2)}) collective-permute-start(bf16[1584,128]{1,0:T(8,128)(2,1)S(1)} %get-tuple-element.44), channel_id=1, source_target_pairs={{0,24},{8,16},{16,8},{24,0},{1,25},{9,17},{17,9},{25,1},{2,26},{10... | collective-permute-start | bytes 1216520 | tf_op jit(solution)/shard_map/ppermute | solution.py:158
  25.8 2.0 collective-permute-start
  27.8 0.7 reshape.211
  28.5 43.6 %all-to-all-start.1 = ((bf16[8,4,1408]{2,1,0:T(4,128)(2,1)}), bf16[8,4,1408]{2,1,0:T(4,128)(2,1)S(1)}, u32[]{:S(2)}, u32[]{:S(2)}) async-start(bf16[8,4,1408]{2,1,0:T(4,128)(2,1)} %reshape.211), calls=%async_computation.1 | async-start | bytes 180224 | tf_op jit(solution)/shard_map/all_to_all | solution.py:23
  72.8 0.4 copy.79
  73.4 20.9 %all-to-all-done.1 = bf16[8,4,1408]{2,1,0:T(4,128)(2,1)S(1)} async-done(((bf16[8,4,1408]{2,1,0:T(4,128)(2,1)}), bf16[8,4,1408]{2,1,0:T(4,128)(2,1)S(1)}, u32[]{:S(2)}, u32[]{:S(2)}) %all-to-all-start.1) | async-done | bytes 90144 | tf_op jit(solution)/shard_map/all_to_all | solution.py:23
  94.8 0.3 multiply_reduce_fusion
  95.8 0.6 broadcast_in_dim.55
  96.4 13.3 %all-to-all-start.2 = ((bf16[8,4,512]{2,1,0:T(4,128)(2,1)}), bf16[8,4,512]{2,1,0:T(4,128)(2,1)S(1)}, u32[]{:S(2)}, u32[]{:S(2)}) async-start(bf16[8,4,512]{2,1,0:T(4,128)(2,1)} %broadcast_in_dim.55), calls=%async_computation.2 | async-start | bytes 65536 | tf_op jit(solution)/shard_map/all_to_all | solution.py:28
  109.7 1.3 multiply_add_fusion
  111.0 20.1 %all-to-all-done.2 = bf16[8,4,512]{2,1,0:T(4,128)(2,1)S(1)} async-done(((bf16[8,4,512]{2,1,0:T(4,128)(2,1)}), bf16[8,4,512]{2,1,0:T(4,128)(2,1)S(1)}, u32[]{:S(2)}, u32[]{:S(2)}) %all-to-all-start.2) | async-done | bytes 32800 | tf_op jit(solution)/shard_map/all_to_all | solution.py:28
  132.2 16.5 %all_to_all.45 = bf16[8,32,640]{2,1,0:T(8,128)(2,1)S(1)} all-to-all(bf16[8,32,640]{2,1,0:T(8,128)(2,1)S(1)} %broadcast_in_dim.59), channel_id=1, replica_groups=mesh['grp'=2,'far'=8,'near'=4,'tp'=8] {'tp'}, dimensions={0} | all-to-all | bytes 655360 | tf_op jit(solution)/shard_map/all_to_all | solution.py:28
  148.9 19.8 %all_to_all.46 = bf16[4,32,512]{2,1,0:T(8,128)(2,1)S(1)} all-to-all(bf16[4,32,512]{2,1,0:T(8,128)(2,1)S(1)} %broadcast_in_dim.60), channel_id=1, replica_groups=mesh['grp'=2,'far'=8,'near'=4,'tp'=8] {'near'}, dimensions={0} | all-to-all | bytes 262144 | tf_op jit(solution)/shard_map/all_to_all | solution.py:28
  169.4 31.2 %all_to_all.47 = bf16[8,16,640]{2,1,0:T(8,128)(2,1)S(1)} all-to-all(bf16[8,16,640]{2,1,0:T(8,128)(2,1)S(1)} %bitcast.181), channel_id=1, replica_groups=mesh['grp'=2,'far'=8,'near'=4,'tp'=8] {'far'}, dimensions={0} | all-to-all | bytes 327680 | tf_op jit(solution)/shard_map/all_to_all | solution.py:23
  200.9 31.6 %all_to_all.48 = bf16[8,16,512]{2,1,0:T(8,128)(2,1)S(1)} all-to-all(bf16[8,16,512]{2,1,0:T(8,128)(2,1)S(1)} %broadcast_in_dim.71), channel_id=1, replica_groups=mesh['grp'=2,'far'=8,'near'=4,'tp'=8] {'far'}, dimensions={0} | all-to-all | bytes 262144 | tf_op jit(solution)/shard_map/all_to_all | solution.py:28
  233.2 10.4 %all_to_all.49 = bf16[4,128,128]{2,1,0:T(8,128)(2,1)S(1)} all-to-all(bf16[4,128,128]{2,1,0:T(8,128)(2,1)S(1)} %pad_maximum_fusion.3), channel_id=1, replica_groups=mesh['grp'=2,'far'=8,'near'=4,'tp'=8] {'near'}, dimensions={0} | all-to-all | bytes 262144 | tf_op jit(solution)/shard_map/all_to_all | solution.py:239
  243.6 14.2 %all_to_all.50 = bf16[8,128,128]{2,1,0:T(8,128)(2,1)S(1)} all-to-all(bf16[8,128,128]{2,1,0:T(8,128)(2,1)S(1)} %broadcast_in_dim.72), channel_id=1, replica_groups=mesh['grp'=2,'far'=8,'near'=4,'tp'=8] {'tp'}, dimensions={0} | all-to-all | bytes 524288 | tf_op jit(solution)/shard_map/all_to_all | solution.py:28
  257.9 0.6 copy.88
  (108 shorter events, 5.6 us)
Async XLA Ops:
  0.6 12.8 %copy-start.11 = (s32[4]{0:T(128)S(1)}, s32[4]{0:T(128)}, u32[]{:S(2)}) copy-start(s32[4]{0:T(128)} %param.21) | copy-start | bytes 52
  0.6 13.0 %copy-start.8 = (bf16[512]{0:T(512)(128)(2,1)S(1)}, bf16[512]{0:T(512)(128)(2,1)}, u32[]{:S(2)}) copy-start(bf16[512]{0:T(512)(128)(2,1)} %param.35) | copy-start | bytes 3076
  2.8 15.5 %all-to-all-start = ((bf16[4,32,1408]{2,1,0:T(8,128)(2,1)}), bf16[4,32,1408]{2,1,0:T(8,128)(2,1)S(1)}, u32[]{:S(2)}, u32[]{:S(2)}) async-start(bf16[4,32,1408]{2,1,0:T(8,128)(2,1)} %bitcast.186), calls=%async_computation | async-start | bytes 720896 | tf_op jit(solution)/shard_map/all_to_all | solution.py:23
  11.8 1.9 copy-start.1
  13.3 0.9 copy-start.2
  13.5 0.9 copy-start.3
  13.5 0.9 copy-start.7
  13.5 0.9 copy-start.4
  13.5 0.9 copy-start.6
  13.7 4.7 %copy-start.9 = (bf16[128]{0:T(256)(128)(2,1)S(1)}, bf16[128]{0:T(256)(128)(2,1)}, u32[]{:S(2)}) copy-start(bf16[128]{0:T(256)(128)(2,1)} %param.37) | copy-start | bytes 772
  18.4 9.3 %copy-start.12 = (f32[8]{0:T(128)S(1)}, f32[8]{0:T(128)}, u32[]{:S(2)}) copy-start(f32[8]{0:T(128)} %param.32) | copy-start | bytes 100
  18.4 9.3 %copy-start.5 = (bf16[4,3,512]{2,0,1:T(4,128)(2,1)S(1)}, bf16[4,3,512]{2,0,1:T(4,128)(2,1)}, u32[]{:S(2)}) copy-start(bf16[4,3,512]{2,0,1:T(4,128)(2,1)} %param.22) | copy-start | bytes 36868
  18.5 53.6 %collective-permute-start.1 = (bf16[1584,128]{1,0:T(8,128)(2,1)S(1)}, bf16[1584,128]{1,0:T(8,128)(2,1)S(1)}, u32[]{:S(2)}, u32[]{:S(2)}) collective-permute-start(bf16[1584,128]{1,0:T(8,128)(2,1)S(1)} %get-tuple-element.45), channel_id=1, source_target_pairs={{0,16},{8,24},{16,0},{24,8},{1,17},{9,25},{17,1},{25,9},{2,18},{10... | collective-permute-start | bytes 1216520 | tf_op jit(solution)/shard_map/ppermute | solution.py:158
  21.0 51.1 %collective-permute-start.2 = (bf16[1584,128]{1,0:T(8,128)(2,1)S(1)}, bf16[1584,128]{1,0:T(8,128)(2,1)S(1)}, u32[]{:S(2)}, u32[]{:S(2)}) collective-permute-start(bf16[1584,128]{1,0:T(8,128)(2,1)S(1)} %get-tuple-element.44), channel_id=1, source_target_pairs={{0,24},{8,16},{16,8},{24,0},{1,25},{9,17},{17,9},{25,1},{2,26},{10... | collective-permute-start | bytes 1216520 | tf_op jit(solution)/shard_map/ppermute | solution.py:158
  25.8 46.4 %collective-permute-start = (bf16[1584,128]{1,0:T(8,128)(2,1)S(1)}, bf16[1584,128]{1,0:T(8,128)(2,1)S(1)}, u32[]{:S(2)}, u32[]{:S(2)}) collective-permute-start(bf16[1584,128]{1,0:T(8,128)(2,1)S(1)} %get-tuple-element.46), channel_id=1, source_target_pairs={{0,8},{8,0},{16,24},{24,16},{1,9},{9,1},{17,25},{25,17},{2,10},{10... | collective-permute-start | bytes 1216520 | tf_op jit(solution)/shard_map/ppermute | solution.py:158
  28.5 65.8 %all-to-all-start.1 = ((bf16[8,4,1408]{2,1,0:T(4,128)(2,1)}), bf16[8,4,1408]{2,1,0:T(4,128)(2,1)S(1)}, u32[]{:S(2)}, u32[]{:S(2)}) async-start(bf16[8,4,1408]{2,1,0:T(4,128)(2,1)} %reshape.211), calls=%async_computation.1 | async-start | bytes 180224 | tf_op jit(solution)/shard_map/all_to_all | solution.py:23
  73.3 21.5 %copy-start = (f32[4,8,64,128]{3,2,1,0:T(8,128)S(1)}, f32[4,8,64,128]{3,2,1,0:T(8,128)}, u32[]{:S(2)}) copy-start(f32[4,8,64,128]{3,2,1,0:T(8,128)} %param.24) | copy-start | bytes 3145732
  73.3 21.8 %copy-start.10 = (f32[8]{0:T(128)S(1)}, f32[8]{0:T(128)}, u32[]{:S(2)}) copy-start(f32[8]{0:T(128)} %param.31) | copy-start | bytes 100
  96.4 34.7 %all-to-all-start.2 = ((bf16[8,4,512]{2,1,0:T(4,128)(2,1)}), bf16[8,4,512]{2,1,0:T(4,128)(2,1)S(1)}, u32[]{:S(2)}, u32[]{:S(2)}) async-start(bf16[8,4,512]{2,1,0:T(4,128)(2,1)} %broadcast_in_dim.55), calls=%async_computation.2 | async-start | bytes 65536 | tf_op jit(solution)/shard_map/all_to_all | solution.py:28
